TPU v7x, 768 devices: a whole 4x8x12 slice. The times are simulated.
768 devices in a mesh: sp: 96 (over z, y), tp: 8 (over x, core).
Axes of the slice: x: 4, y: 8, z: 12, core: 2. Of those that a mesh axis runs over, the one named last changes fastest.
Arguments:
- latents: bfloat16 [61440, 2048], P('sp'), may hold values from -6 to 6
- cond: float32 [2048], replicated, may hold values from -6 to 6
- ctx_cond: float32 [2048], replicated, may hold values from -6 to 6
- context: bfloat16 [768, 2048], P('sp'), may hold values from -6 to 6
- norm_gain: float32 [2048], replicated, may hold values from 0.1 to 1.9
- shift_weight: bfloat16 [2048, 2048], P('tp'), may hold values from -0.125 to 0.125
- scale_weight: bfloat16 [2048, 2048], P('tp'), may hold values from -0.125 to 0.125
- gate_weight: bfloat16 [2048, 2048], P('tp'), may hold values from -0.125 to 0.125
- q_weight: bfloat16 [2048, 1024], P(None, 'tp'), may hold values from -0.125 to 0.125
- k_weight: bfloat16 [2048, 1024], P(None, 'tp'), may hold values from -0.125 to 0.125
- v_weight: bfloat16 [2048, 1024], P(None, 'tp'), may hold values from -0.125 to 0.125
- out_weight: bfloat16 [1024, 2048], replicated, may hold values from -1.5 to 1.5
- rel_bias: float32 [8, 15, 31], P('tp'), may hold values from 1.5 to 260
Outputs:
- result: bfloat16 [61440, 2048], P(('sp', 'tp'))
All inputs are finite; a program needn't handle non-finite values.
Results may differ from a plain program's by a relative error of at most 0.0085.
Values may be sent and summed in bfloat16 or wider, within the bound.
A program may use at most 64 MiB of HBM per device.

v0:
```python
import jax
import jax.numpy as jnp
from jax import lax
from jax.sharding import PartitionSpec as P

HEAD_DIM = 128
GRID_W = 64
WIN_ROWS = 8
WIN_COLS = 16


EPS = 1e-06
NEG_BIG = -1e30


def from_everyone(shard, axis):
    count = lax.axis_size(axis)
    return lax.all_to_all(
        jnp.broadcast_to(shard[None], (count, *shard.shape)), axis, 0, 0, tiled=True
    )


def over_copies(shard, axis):
    return from_everyone(shard, axis).sum(axis=0)


def together(arrays, axis):
    ravelled, at, outs = (jnp.concatenate([a.reshape(-1) for a in arrays]), 0, [])
    subtotal = over_copies(ravelled, axis)
    for a in arrays:
        outs.append(subtotal[at : at + a.size].reshape(a.shape))
        at += a.size
    return tuple(outs)


def sent_together(arrays, axis, dim, along):
    widths = [a.shape[along] for a in arrays]
    both = jnp.concatenate(arrays, axis=along)
    whole = lax.all_gather(both, axis, axis=dim, tiled=True)
    return tuple(jnp.split(whole, [sum(widths[:k]) for k in range(1, len(widths))], axis=along))


def with_halo(shard, sides, width):
    for axis, dim in sides:
        count, length = (lax.axis_size(axis), shard.shape[dim])
        up = [(i, (i + 1) % count) for i in range(count - 1)]
        down = [(j, i) for i, j in up]
        last = lax.slice_in_dim(shard, length - width, length, axis=dim)
        initial = lax.slice_in_dim(shard, 0, width, axis=dim)
        before = lax.ppermute(last, axis, up)
        after = lax.ppermute(initial, axis, down)
        shard = jnp.concatenate([before, shard, after], axis=dim)
    return shard


def modulated_norm(tok_rows, gain, shift_row, scale_row):
    rows_f = tok_rows.astype(jnp.float32)
    inverse = lax.rsqrt(jnp.mean(rows_f * rows_f, axis=-1, keepdims=True) + EPS)
    return (rows_f * inverse * gain * (1.0 + scale_row) + shift_row).astype(jnp.bfloat16)


def column_mask():
    columns = jnp.arange(GRID_W, dtype=jnp.int32)
    first_col = jnp.clip(columns - WIN_COLS // 2, 0, GRID_W - WIN_COLS)
    inside = (columns[None, :] >= first_col[:, None]) & (
        columns[None, :] < first_col[:, None] + WIN_COLS
    )
    return jnp.tile(inside, (1, WIN_ROWS))


def grid_bias(bias_table, row_diff):
    row_hot = (
        row_diff[:, :, None] == jnp.arange(2 * WIN_ROWS - 1, dtype=jnp.int32)[None, None, :]
    ).astype(jnp.float32)
    columns = jnp.arange(GRID_W, dtype=jnp.int32)
    col_diff = (
        jnp.clip(columns[None, :] - columns[:, None], -(WIN_COLS - 1), WIN_COLS - 1) + WIN_COLS - 1
    )
    col_hot = (
        col_diff[:, :, None] == jnp.arange(2 * WIN_COLS - 1, dtype=jnp.int32)[None, None, :]
    ).astype(jnp.float32)
    middle = jnp.einsum("rai,hij->hraj", row_hot, bias_table, precision=lax.Precision.HIGHEST)
    spread = jnp.einsum("hraj,qbj->hrqab", middle, col_hot, precision=lax.Precision.HIGHEST)
    return spread.reshape(bias_table.shape[0], row_diff.shape[0], GRID_W, WIN_ROWS * GRID_W)


def attend(query, key_win, val_win, ctx_keys, ctx_vals, bias, inside):
    factor = HEAD_DIM ** (-0.5)
    near_scores = (
        jnp.einsum("rqhd,rkhd->hrqk", query, key_win, preferred_element_type=jnp.float32) * factor
        + bias
    )
    near_scores = jnp.where(inside, near_scores, NEG_BIG)
    far_scores = (
        jnp.einsum("rqhd,lhd->hrql", query, ctx_keys, preferred_element_type=jnp.float32) * factor
    )
    row_peak = jnp.maximum(
        jnp.max(near_scores, axis=-1, keepdims=True), jnp.max(far_scores, axis=-1, keepdims=True)
    )
    near_exp = jnp.exp(near_scores - row_peak)
    far_exp = jnp.exp(far_scores - row_peak)
    denominator = jnp.sum(near_exp, axis=-1, keepdims=True) + jnp.sum(
        far_exp, axis=-1, keepdims=True
    )
    near_w = (near_exp / denominator).astype(jnp.bfloat16)
    far_w = (far_exp / denominator).astype(jnp.bfloat16)
    mixed = jnp.einsum(
        "hrqk,rkhd->rqhd", near_w, val_win, preferred_element_type=jnp.float32
    ) + jnp.einsum("hrql,lhd->rqhd", far_w, ctx_vals, preferred_element_type=jnp.float32)
    return mixed.astype(jnp.bfloat16)


def shards(
    latents,
    cond,
    ctx_cond,
    context,
    norm_gain,
    shift_weight,
    scale_weight,
    gate_weight,
    q_weight,
    k_weight,
    v_weight,
    out_weight,
    rel_bias,
):
    tp_rows = shift_weight.shape[0]
    conds = jnp.stack([cond, ctx_cond])
    active = jax.nn.silu(
        lax.dynamic_slice_in_dim(conds, lax.axis_index("tp") * tp_rows, tp_rows, 1)
    ).astype(jnp.bfloat16)
    shifts = jnp.dot(active, shift_weight, preferred_element_type=jnp.float32)
    scales = jnp.dot(active, scale_weight, preferred_element_type=jnp.float32)
    gates = jnp.dot(active[:1], gate_weight, preferred_element_type=jnp.float32)
    shifts, scales, gates = together((shifts, scales, gates), "tp")
    tok_dev = latents.shape[0]
    heads_here = q_weight.shape[1] // HEAD_DIM
    rows_here = tok_dev // GRID_W
    h_lat = modulated_norm(latents, norm_gain, shifts[0], scales[0])
    query = jnp.dot(h_lat, q_weight, preferred_element_type=jnp.float32).astype(jnp.bfloat16)
    keys = jnp.dot(h_lat, k_weight, preferred_element_type=jnp.float32).astype(jnp.bfloat16)
    values = jnp.dot(h_lat, v_weight, preferred_element_type=jnp.float32).astype(jnp.bfloat16)
    h_ctx = modulated_norm(context, norm_gain, shifts[1], scales[1])
    own_keys = jnp.dot(h_ctx, k_weight, preferred_element_type=jnp.float32).astype(jnp.bfloat16)
    own_vals = jnp.dot(h_ctx, v_weight, preferred_element_type=jnp.float32).astype(jnp.bfloat16)
    ctx_keys, ctx_vals = sent_together((own_keys, own_vals), "sp", 0, 1)
    ctx_count = ctx_keys.shape[0]
    ctx_keys = ctx_keys.reshape(ctx_count, heads_here, HEAD_DIM)
    ctx_vals = ctx_vals.reshape(ctx_count, heads_here, HEAD_DIM)
    half_rows = WIN_ROWS // 2
    stacked = jnp.stack([keys, values]).reshape(2, rows_here, GRID_W, heads_here * HEAD_DIM)
    padded = with_halo(stacked, (("sp", 1),), half_rows)
    base_row = lax.axis_index("sp") * rows_here
    total_rows = rows_here * lax.axis_size("sp")
    grid_rows = base_row + jnp.arange(rows_here, dtype=jnp.int32)
    first_row = jnp.clip(grid_rows - half_rows, 0, total_rows - WIN_ROWS)
    offsets = jnp.arange(WIN_ROWS, dtype=jnp.int32)
    local_index = (first_row - base_row + half_rows)[:, None] + offsets[None, :]
    windows = padded[:, local_index].reshape(2, rows_here, WIN_ROWS * GRID_W, heads_here, HEAD_DIM)
    row_diff = first_row[:, None] + offsets[None, :] - grid_rows[:, None] + WIN_ROWS - 1
    bias = grid_bias(rel_bias, row_diff)
    query_grid = query.reshape(rows_here, GRID_W, heads_here, HEAD_DIM)
    attn = attend(query_grid, windows[0], windows[1], ctx_keys, ctx_vals, bias, column_mask())
    attn = attn.reshape(tok_dev, heads_here * HEAD_DIM)
    own_rows = lax.all_to_all(attn, "tp", split_axis=0, concat_axis=1, tiled=True)
    row_count = own_rows.shape[0]
    residual = lax.dynamic_slice_in_dim(latents, lax.axis_index("tp") * row_count, row_count, 0)
    mixed = jnp.dot(own_rows, out_weight, preferred_element_type=jnp.float32)
    return (residual.astype(jnp.float32) + gates[0] * mixed).astype(jnp.bfloat16)


def solution(mesh):
    in_specs = (
        P("sp", None),
        P(),
        P(),
        P("sp", None),
        P(),
        P("tp", None),
        P("tp", None),
        P("tp", None),
        P(None, "tp"),
        P(None, "tp"),
        P(None, "tp"),
        P(),
        P("tp", None, None),
    )
    out_specs = P(("sp", "tp"), None)
    return jax.shard_map(shards, mesh=mesh, in_specs=in_specs, out_specs=out_specs, check_vma=False)
```

profile of v0, /device:TPU:1, one launch (start us, length us, event | category | flops | bytes accessed | tf_op | source)
XLA Modules:
  0.0 139.1 jit_solution(4765112239642208792)
XLA Ops:
  0.0 0.9 fusion.31
  0.9 0.3 copy-done
  1.3 0.2 convolution_bitcast_fusion.5
  1.5 1.5 %convolution_bitcast_fusion.4 = f32[1,16,2,128]{3,2,1,0:T(2,128)S(1)} fusion(bf16[2,256]{1,0:T(2,128)(2,1)S(1)} %fusion.31, bf16[256,2048]{1,0:T(8,128)(2,1)} %param.19), kind=kOutput, calls=%fused_computation.31 | convolution fusion | flops 2097152 | bytes 1065984 | tf_op jit(solution)/shard_map/dot_general | solution.py:134
  3.0 0.2 fusion.32
  3.3 0.9 broadcast_in_dim.8
  4.2 13.8 %all-to-all-start = ((f32[8,1,10240]{2,1,0:T(1,128)}), f32[8,1,10240]{2,1,0:T(1,128)S(1)}, u32[]{:S(2)}, u32[]{:S(2)}) async-start(f32[8,1,10240]{2,1,0:T(1,128)} %broadcast_in_dim.8), calls=%async_computation | async-start | bytes 655360 | tf_op jit(solution)/shard_map/all_to_all | solution.py:18
  18.0 2.3 %fusion = f32[640]{0:T(1024)S(1)} fusion(bf16[640,2048]{1,0:T(8,128)(2,1)} %param.13), kind=kLoop, calls=%fused_computation.3 | loop fusion | flops 3931520 | bytes 2624000 | tf_op jit(solution)/shard_map/reduce_sum | solution.py:58
  20.8 1.8 %convolution_bitcast_fusion = f32[1,10,64,8,64]{4,1,3,2,0:T(8,128)S(1)} fusion(f32[10,8,31,1]{2,0,1,3:T(8,128)S(1)} %convolution_bitcast_fusion.3, s32[64,64]{1,0:T(8,128)S(1)} %clamp_add_fusion), kind=kOutput, calls=%fused_computation.12 | convolution fusion | flops 122023936 | bytes 1337024 | tf_op jit(solution)/shard_map/hraj,qbj->hrqab/dot_general | solution.py:83
  22.5 2.3 %copy.27 = f32[1,10,64,8,64]{4,3,2,1,0:T(8,128)} copy(f32[1,10,64,8,64]{4,1,3,2,0:T(8,128)S(1)} %convolution_bitcast_fusion) | data formatting | bytes 2621440 | tf_op jit(solution)/shard_map/hraj,qbj->hrqab/transpose | solution.py:83
  24.9 2.1 %reshape.307 = f32[10,64,512]{2,1,0:T(8,128)S(1)} reshape(f32[1,10,64,8,64]{4,3,2,1,0:T(8,128)} %copy.27) | data formatting | bytes 2621440 | tf_op jit(solution)/shard_map/reshape | solution.py:84
  27.4 0.2 reduce_sum.45
  27.7 2.8 %fusion.4 = bf16[640,2048]{1,0:T(8,128)(2,1)S(1)} fusion(bf16[640,2048]{1,0:T(8,128)(2,1)} %param.13, f32[2048]{0:T(1024)S(1)} %get-tuple-element.10, f32[2048]{0:T(1024)S(1)} %get-tuple-element.11, f32[2048]{0:T(1024)S(1)} %copy-done.6, f32[640]{0:T(1024)S(1)} %add_rsqrt_fusion), kind=kLoop, calls=%fused_computation.7 | loop fusion | flops 7864320 | bytes 5270016 | tf_op jit(solution)/shard_map/convert_element_type | solution.py:59
  30.5 0.8 convolution_convert_fusion.2
  31.6 0.8 convolution_convert_fusion.1
  32.9 1.3 collective-permute-start
  34.2 1.3 collective-permute-start.1
  35.5 0.8 convolution_convert_fusion
  36.4 58.6 %all_gather.3 = bf16[768,256]{1,0:T(8,128)(2,1)S(1)} all-gather(bf16[8,256]{1,0:T(8,128)(2,1)S(1)} %pad_maximum_fusion.4), channel_id=1, replica_groups=mesh['sp'=96,'tp'=8] {'sp'}, dimensions={0}, use_global_device_ids=true | all-gather | bytes 397312 | tf_op jit(solution)/shard_map/all_gather | solution.py:39
  95.0 2.3 %multiply_reduce_fusion = (f32[10,64]{1,0:T(8,128)}, f32[10,64,768]{2,1,0:T(8,128)}) fusion(bf16[10,64,128]{2,1,0:T(8,128)(2,1)S(1)} %bitcast.91, bf16[768,256]{1,0:T(8,128)(2,1)S(1)} %all_gather.3), kind=kOutput, calls=%fused_computation.15 | convolution fusion | flops 126811520 | bytes 2329088 | tf_op jit(solution)/shard_map/rqhd,lhd->hrql/dot_general | solution.py:95
  97.4 2.5 %gather_fusion = bf16[80,2,64,128]{3,2,1,0:T(8,128)(2,1)} fusion(bf16[2,18,64,128]{3,2,1,0:T(8,128)(2,1)S(1)} %pad_maximum_fusion, s32[1024]{0:T(1024)S(1)} %pad_clamp_fusion), kind=kCustom, calls=%fused_computation | custom fusion | bytes 5243200 | tf_op jit(solution)/shard_map/gather | solution.py:160
  100.0 2.3 %copy.49 = bf16[10,8,2,64,128]{4,3,1,0,2:T(8,128)(2,1)S(1)} copy(bf16[10,8,2,64,128]{4,3,2,1,0:T(8,128)(2,1)} %bitcast.88) | data formatting | bytes 5242880 | tf_op jit(solution)/shard_map/gather | solution.py:160
  102.3 0.8 fusion.36
  103.1 0.7 fusion.37
  103.8 0.8 copy-done.1
  104.6 0.5 fusion.7
  105.1 0.5 fusion.12
  105.6 0.5 convolution_bitcast_fusion.2
  106.1 1.3 fusion.11
  107.4 22.3 %all-to-all-start.1 = ((bf16[8,80,128]{2,1,0:T(8,128)(2,1)}), bf16[8,80,128]{2,1,0:T(8,128)(2,1)S(1)}, u32[]{:S(2)}, u32[]{:S(2)}) async-start(bf16[8,80,128]{2,1,0:T(8,128)(2,1)} %bitcast.21), calls=%async_computation.1 | async-start | bytes 327680 | tf_op jit(solution)/shard_map/all_to_all | solution.py:166
  129.7 5.5 %all-to-all-done.1 = bf16[8,80,128]{2,1,0:T(8,128)(2,1)S(1)} async-done(((bf16[8,80,128]{2,1,0:T(8,128)(2,1)}), bf16[8,80,128]{2,1,0:T(8,128)(2,1)S(1)}, u32[]{:S(2)}, u32[]{:S(2)}) %all-to-all-start.1) | async-done | bytes 163872 | tf_op jit(solution)/shard_map/all_to_all | solution.py:166
  135.3 3.8 %fusion.6 = bf16[80,2048]{1,0:T(8,128)(2,1)} fusion(bf16[1024,2048]{1,0:T(8,128)(2,1)} %param.24, f32[2048]{0:T(1024)S(1)} %get-tuple-element.12, bf16[640,2048]{1,0:T(8,128)(2,1)} %param.13, s32[]{:T(128)S(6)} %select_n.21, bf16[8,80,128]{2,1,0:T(8,128)(2,1)S(1)} %all-to-all-done.1), kind=kOutput, calls=%fused_computation.11 | convolution fusion | flops 336199680 | bytes 5021700 | tf_op jit(solution)/shard_map/dot_general | solution.py:169
  (47 shorter events, 1.7 us)
Async XLA Ops:
  0.0 1.3 copy-start
  0.0 3.0 %copy-start.2 = (bf16[256,2048]{1,0:T(8,128)(2,1)S(1)}, bf16[256,2048]{1,0:T(8,128)(2,1)}, u32[]{:S(2)}) copy-start(bf16[256,2048]{1,0:T(8,128)(2,1)} %param.20) | copy-start | bytes 3145732
  3.2 17.3 %copy-start.8 = (f32[1,15,31]{2,0,1:T(1,128)S(1)}, f32[1,15,31]{2,0,1:T(1,128)}, u32[]{:S(2)}) copy-start(f32[1,15,31]{2,0,1:T(1,128)} %param.25) | copy-start | bytes 5584
  4.2 23.2 %all-to-all-start = ((f32[8,1,10240]{2,1,0:T(1,128)}), f32[8,1,10240]{2,1,0:T(1,128)S(1)}, u32[]{:S(2)}, u32[]{:S(2)}) async-start(f32[8,1,10240]{2,1,0:T(1,128)} %broadcast_in_dim.8), calls=%async_computation | async-start | bytes 655360 | tf_op jit(solution)/shard_map/all_to_all | solution.py:18
  24.9 2.4 %copy-start.5 = (bf16[8,2048]{1,0:T(8,128)(2,1)S(1)}, bf16[8,2048]{1,0:T(8,128)(2,1)}, u32[]{:S(2)}) copy-start(bf16[8,2048]{1,0:T(8,128)(2,1)} %param.16) | copy-start | bytes 98308
  24.9 2.8 %copy-start.6 = (f32[2048]{0:T(1024)S(1)}, f32[2048]{0:T(1024)}, u32[]{:S(2)}) copy-start(f32[2048]{0:T(1024)} %param.17) | copy-start | bytes 24580
  27.7 2.9 %copy-start.4 = (bf16[2048,128]{1,0:T(8,128)(2,1)S(1)}, bf16[2048,128]{1,0:T(8,128)(2,1)}, u32[]{:S(2)}) copy-start(bf16[2048,128]{1,0:T(8,128)(2,1)} %param.22) | copy-start | bytes 1572868
  30.5 1.0 copy-start.3
  31.6 4.0 %copy-start.9 = (bf16[2048,128]{1,0:T(8,128)(2,1)S(1)}, bf16[2048,128]{1,0:T(8,128)(2,1)}, u32[]{:S(2)}) copy-start(bf16[2048,128]{1,0:T(8,128)(2,1)} %param.21) | copy-start | bytes 1572868
  32.9 64.4 %collective-permute-start = (bf16[2,4,64,128]{3,2,1,0:T(8,128)(2,1)S(1)}, bf16[2,4,64,128]{3,2,1,0:T(8,128)(2,1)S(1)}, u32[]{:S(2)}, u32[]{:S(2)}) collective-permute-start(bf16[2,4,64,128]{3,2,1,0:T(8,128)(2,1)S(1)} %get-tuple-element.7), channel_id=1, source_target_pairs={{0,8},{8,16},{16,24},{24,32},{32,40},{40,48},{48,56},{56,64},{64,7... | collective-permute-start | bytes 393224 | tf_op jit(solution)/shard_map/ppermute | solution.py:50
  34.2 63.1 %collective-permute-start.1 = (bf16[2,4,64,128]{3,2,1,0:T(8,128)(2,1)S(1)}, bf16[2,4,64,128]{3,2,1,0:T(8,128)(2,1)S(1)}, u32[]{:S(2)}, u32[]{:S(2)}) collective-permute-start(bf16[2,4,64,128]{3,2,1,0:T(8,128)(2,1)S(1)} %get-tuple-element.8), channel_id=1, source_target_pairs={{8,0},{16,8},{24,16},{32,24},{40,32},{48,40},{56,48},{64,56},{72,6... | collective-permute-start | bytes 393224 | tf_op jit(solution)/shard_map/ppermute | solution.py:51
  103.0 0.7 copy-start.7
  103.1 1.6 %copy-start.1 = (f32[10,64,768]{2,1,0:T(8,128)S(1)}, f32[10,64,768]{2,1,0:T(8,128)}, u32[]{:S(2)}) copy-start(f32[10,64,768]{2,1,0:T(8,128)} %get-tuple-element.17) | copy-start | bytes 5898244
  107.4 27.9 %all-to-all-start.1 = ((bf16[8,80,128]{2,1,0:T(8,128)(2,1)}), bf16[8,80,128]{2,1,0:T(8,128)(2,1)S(1)}, u32[]{:S(2)}, u32[]{:S(2)}) async-start(bf16[8,80,128]{2,1,0:T(8,128)(2,1)} %bitcast.21), calls=%async_computation.1 | async-start | bytes 327680 | tf_op jit(solution)/shard_map/all_to_all | solution.py:166
where the time goes:
time: 140 us; the launch traced here: 139 us
  blocking collectives  58.6 us (42%)
  starting transfers between devices  38.7 us (28%)
  matrix products  15.6 us (11%)
  local copies, waits for them, and re-layouts  12.6 us (9%)
  other arithmetic  7.76 us (6%)
  waiting for transfers between devices  5.56 us (4%)
    all_gather x1, blocking collectives, sent_together(): whole = lax.all_gather(both, axis, axis=dim, tiled=True)  58.6 us
    all_to_all x1, starting transfers between devices, shards(): lax.all_to_all(attn, 'tp', split_axis=0, concat_axis=1, tiled=True)  22.3 us
    all_to_all x1, starting transfers between devices, from_everyone(): lax.all_to_all(jnp.broadcast_to(shard[None], (count, *shard.shape)), axis...  13.8 us
    all_to_all x1, waiting for transfers between devices, shards(): lax.all_to_all(attn, 'tp', split_axis=0, concat_axis=1, tiled=True)  5.55 us
    gather x2, local copies, waits for them, and re-layouts, shards(): padded[:, local_index]  4.84 us
    dot_general x1, matrix products, shards(): mixed = jnp.dot(own_rows, out_weight, preferred_element_type=jnp.float32)  3.83 us
    convert_element_type x1, other arithmetic, modulated_norm(): (rows_f * inverse * gain * (1.0 + scale_row) + shift_row).astype(jnp.bflo...  2.83 us
  transfers between devices with their start and end apart: 4, of which 1 were waited for; matrix products, arithmetic and copies ran while one was open for 9% of the time, Pallas kernels for 0%

commit v1 on v0

v1 whole, which is shorter than its diff:
```python
import jax
import jax.numpy as jnp
from jax import lax
from jax.experimental import pallas as pl
from jax.experimental.pallas import tpu as pltpu
from jax.sharding import PartitionSpec as P

D = 2048
HD = 128
GW = 64
WR = 8
WC = 16
EPS = 1e-06
NEG = -1e30
ZN, YN, XN = 12, 8, 4
NT = D // 128
TOK = 640
ROWS = TOK // GW
ALL_ROWS = ROWS * ZN * YN
BEFORE, AFTER = 4, 3
OWN = BEFORE * GW
KVN = (BEFORE + ROWS + AFTER) * GW
CR = 8
CB = CR * ZN
F32 = jnp.float32
BF16 = jnp.bfloat16
NT_DIMS = (((1,), (1,)), ((), ()))


def body(
    lat_h, cond_h, cctx_h, ctx_h, gain_h, shw_h, scw_h, gtw_h, qw_h, kw_h, vw_h, ow_h, rb_h,
    out_ref,
    lat, cond, cctx, craw, gain, mw, w, wo, rb,
    part, recva, red, mod, inv, tabs, bias, hbuf, qb, kv, cown, cslot,
    mwin, lwin, owin, attn, own, acc,
    in_sem, a_sem, bs_sem, br_sem, zs_sem, zr_sem, f_sem, ys_sem, yr_sem, h_sem, os_sem, or_sem,
):
    s = lax.axis_index("sp")
    t = lax.axis_index("tp")
    z, y = s // YN, s % YN
    x, c = t // 2, t % 2

    def tp_of(dx, f):
        return lax.rem(x + dx, XN) * 2 + (c if f == 0 else 1 - c)

    tp_peers = [(dx, f) for dx in (2, 1, 3, 0) for f in (0, 1) if (dx, f) != (0, 0)]
    z_order = sorted(range(1, ZN), key=lambda d: -min(d, ZN - d))
    y_order = sorted(range(1, YN), key=lambda d: -min(d, YN - d))

    loads = {}

    def load(name, k, src, dst):
        loads[name] = pltpu.make_async_copy(src, dst, in_sem.at[k])
        loads[name].start()

    load("cond", 0, cond_h, cond)
    load("cctx", 1, cctx_h, cctx)
    load("sc", 2, scw_h, mw.at[0])
    load("sh", 3, shw_h, mw.at[1])
    load("gt", 4, gtw_h, mw.at[2])
    load("ctx", 5, ctx_h, craw.at[0])
    load("rb", 6, rb_h, rb)
    load("gain", 7, gain_h, gain)
    load("lat", 8, lat_h, lat)
    load("qw", 9, qw_h, w.at[:, 0:128])
    load("kw", 10, kw_h, w.at[:, 128:256])
    load("vw", 11, vw_h, w.at[:, 256:384])
    load("ow", 12, ow_h, wo)

    barrier = pltpu.get_barrier_semaphore()

    def hello(sp, tp):
        pl.semaphore_signal(
            barrier, inc=1, device_id={"sp": sp, "tp": tp}, device_id_type=pl.DeviceIdType.MESH
        )

    def sp_z(d):
        return lax.rem(z + d, ZN) * YN + y

    def sp_y(d):
        return z * YN + lax.rem(y + d, YN)

    for d in z_order:
        hello(sp_z(d), t)
    for d in y_order:
        hello(sp_y(d), t)
    for dx, f in tp_peers:
        hello(s, tp_of(dx, f))
    has_next = s < ZN * YN - 1
    has_prev = s > 0
    next_far = jnp.logical_and(y == YN - 1, has_next)
    prev_far = jnp.logical_and(y == 0, has_prev)

    @pl.when(next_far)
    def _():
        hello(s + 1, t)

    @pl.when(prev_far)
    def _():
        hello(s - 1, t)

    def rcopy(src, dst, ssem, rsem, sp, tp):
        return pltpu.make_async_remote_copy(
            src_ref=src, dst_ref=dst, send_sem=ssem, recv_sem=rsem,
            device_id={"sp": sp, "tp": tp}, device_id_type=pl.DeviceIdType.MESH,
        )

    loads["cond"].wait()
    loads["cctx"].wait()

    def silu_row(ref):
        v = jnp.concatenate([ref[pl.ds(2 * t, 1), :], ref[pl.ds(2 * t + 1, 1), :]], axis=1)
        return (v / (1.0 + jnp.exp(-v))).astype(BF16)

    row = lax.broadcasted_iota(jnp.int32, (16, 256), 0)
    act = jnp.where(
        row == 0, silu_row(cond).astype(F32), jnp.where(row == 1, silu_row(cctx).astype(F32), 0.0)
    ).astype(BF16)
    for k, name in enumerate(("sc", "sh", "gt")):
        loads[name].wait()
        for n in range(8):
            o = jnp.dot(act, mw[k, :, n * 256 : (n + 1) * 256], preferred_element_type=F32)
            for i in range(2):
                j = 2 * n + i
                piece = o[:, i * 128 : (i + 1) * 128]
                for r in range(1 if k == 2 else 2):
                    part[j // 8, 2 * k + r, j % 8 : j % 8 + 1, :] = piece[r : r + 1, :]

    pl.semaphore_wait(
        barrier, ZN - 1 + YN - 1 + 2 * XN - 1 + next_far.astype(jnp.int32) + prev_far.astype(jnp.int32)
    )

    a_copy = rcopy(part.at[1 - c], recva, a_sem.at[0], a_sem.at[1], s, tp_of(0, 1))
    a_copy.start()

    loads["ctx"].wait()
    half = pl.ds(pl.multiple_of(c * 1024, 1024), 1024)
    z_copies = [
        rcopy(craw.at[0, :, half], craw.at[ZN - d, :, half], zs_sem.at[d], zr_sem.at[ZN - d], sp_z(d), t)
        for d in z_order
    ]
    for cp in z_copies:
        cp.start()

    a_copy.wait_recv()
    red[0, 0] = part[c] + recva[...]
    b_copies = [
        rcopy(red.at[0, 0], red.at[dx, f], bs_sem.at[2 * dx + f], br_sem.at[2 * dx + f], s, tp_of(dx, f))
        for dx, f in tp_peers
    ]
    for cp in b_copies:
        cp.start()

    loads["rb"].wait()
    full = jnp.concatenate([rb[0], jnp.zeros((15, 97), F32)], axis=1)
    lane = lax.broadcasted_iota(jnp.int32, (15, 128), 1)
    tabs[0] = pltpu.roll(full, 113, 1)
    tabs[1] = pltpu.roll(full, 49, 1)
    lane = lax.broadcasted_iota(jnp.int32, (1, 128), 1)
    qcol = lax.broadcasted_iota(jnp.int32, (GW, 128), 0)
    kcol = lax.broadcasted_iota(jnp.int32, (GW, 128), 1) % GW
    first = jnp.clip(qcol - WC // 2, 0, GW - WC)
    inside = jnp.logical_and(kcol >= first, kcol < first + WC)
    for a in range(14):
        v = jnp.where(
            jnp.logical_and(lane >= 49, lane <= 79), tabs[1, a + 1 : a + 2, :], tabs[0, a : a + 1, :]
        )
        spread = pltpu.roll(jnp.broadcast_to(v, (GW, 128)), 0, 1, stride=1, stride_axis=0)
        bias[a] = jnp.where(inside, spread, NEG)

    loads["lat"].wait()
    for b in range(TOK // 128):
        rows = slice(b * 128, (b + 1) * 128)
        sq = jnp.zeros((128, 128), F32)
        for j in range(NT):
            v = lat[rows, j * 128 : (j + 1) * 128].astype(F32)
            sq += v * v
        mean = jnp.sum(sq, axis=1, keepdims=True) * (1.0 / D)
        inv[rows, :] = jnp.broadcast_to(lax.rsqrt(mean + EPS), (128, 128))

    for cp in z_copies:
        cp.wait_recv()
    f_copy = rcopy(
        craw.at[1:ZN, :, half], craw.at[1:ZN, :, half], f_sem.at[0], f_sem.at[1], s, tp_of(0, 1)
    )
    f_copy.start()

    for cp in b_copies:
        cp.wait_recv()
    loads["gain"].wait()
    for f in range(2):
        tot = red[0, f] + red[1, f] + red[2, f] + red[3, f]
        hh = c if f == 0 else 1 - c
        gn = gain[pl.ds(pl.multiple_of(hh * 8, 8), 8), :]
        mod[hh, 0] = gn * (1.0 + tot[0])
        mod[hh, 1] = gn * (1.0 + tot[1])
        mod[hh, 2] = tot[2]
        mod[hh, 3] = tot[3]
        mod[hh, 4] = tot[4]

    def mrow(v, j):
        return mod[j // 8, v, j % 8 : j % 8 + 1, :]

    for name in ("qw", "kw", "vw"):
        loads[name].wait()

    def project(r0, n):
        rows = slice(r0, r0 + n)
        for j in range(NT):
            cols = slice(j * 128, (j + 1) * 128)
            v = lat[rows, cols].astype(F32) * inv[rows, :] * mrow(0, j) + mrow(2, j)
            hbuf[rows, cols] = v.astype(BF16)
        o = jnp.dot(hbuf[rows, :], w[...], preferred_element_type=F32).astype(BF16)
        qb[rows, :] = o[:, 0:128]
        kv[0, OWN + r0 : OWN + r0 + n, :] = o[:, 128:256]
        kv[1, OWN + r0 : OWN + r0 + n, :] = o[:, 256:384]

    project(TOK - BEFORE * GW, BEFORE * GW)
    to_next = rcopy(
        kv.at[:, KVN - (BEFORE + AFTER) * GW : KVN - AFTER * GW, :], kv.at[:, 0:OWN, :],
        h_sem.at[0], h_sem.at[1], s + 1, t,
    )

    @pl.when(has_next)
    def _():
        to_next.start()

    project(0, BEFORE * GW)
    to_prev = rcopy(
        kv.at[:, OWN : OWN + AFTER * GW, :], kv.at[:, KVN - AFTER * GW : KVN, :],
        h_sem.at[2], h_sem.at[3], s - 1, t,
    )

    @pl.when(has_prev)
    def _():
        to_prev.start()

    f_copy.wait_recv()
    sq = jnp.zeros((CB, 128), F32)
    for j in range(NT):
        v = craw[:, :, j * 128 : (j + 1) * 128].astype(F32).reshape(CB, 128)
        sq += v * v
    cinv = lax.rsqrt(jnp.sum(sq, axis=1, keepdims=True) * (1.0 / D) + EPS)
    cinv = jnp.broadcast_to(cinv, (CB, 128))
    for j in range(NT):
        cols = slice(j * 128, (j + 1) * 128)
        v = craw[:, :, cols].astype(F32).reshape(CB, 128)
        hbuf[TOK : TOK + CB, cols] = (v * cinv * mrow(1, j) + mrow(3, j)).astype(BF16)
    o = jnp.dot(hbuf[TOK : TOK + CB, :], w[:, 128:384], preferred_element_type=F32).astype(BF16)
    cslot[0, 0] = o[:, 0:128]
    cslot[0, 1] = o[:, 128:256]
    y_copies = [
        rcopy(cslot.at[0], cslot.at[YN - d], ys_sem.at[d], yr_sem.at[YN - d], sp_y(d), t)
        for d in y_order
    ]
    for cp in y_copies:
        cp.start()

    project(BEFORE * GW, TOK - 2 * BEFORE * GW)

    factor = HD ** (-0.5)
    base = s * ROWS

    def window(r):
        g = base + r
        first_row = jnp.clip(g - WR // 2, 0, ALL_ROWS - WR)
        a0 = first_row - g + WR - 1
        k0 = pl.multiple_of((first_row - base + BEFORE) * GW, GW)
        rows = slice(r * GW, (r + 1) * GW)
        keys = kv[0, pl.ds(k0, WR * GW), :]
        vals = kv[1, pl.ds(k0, WR * GW), :]
        sc = lax.dot_general(qb[rows, :], keys, NT_DIMS, preferred_element_type=F32) * factor
        sc = jnp.concatenate(
            [sc[:, i * 128 : (i + 1) * 128] + bias[a0 + 2 * i] for i in range(WR // 2)], axis=1
        )
        m = jnp.max(sc, axis=1, keepdims=True)
        p = jnp.exp(sc - m)
        mwin[rows, :] = jnp.broadcast_to(m, (GW, 128))
        lwin[rows, :] = jnp.broadcast_to(jnp.sum(p, axis=1, keepdims=True), (GW, 128))
        owin[rows, :] = jnp.dot(p.astype(BF16), vals, preferred_element_type=F32)

    for r in range(BEFORE, ROWS - AFTER):
        window(r)

    @pl.when(has_prev)
    def _():
        to_next.wait_recv()

    @pl.when(has_next)
    def _():
        to_prev.wait_recv()

    for r in (*range(BEFORE), *range(ROWS - AFTER, ROWS)):
        window(r)

    for cp in y_copies:
        cp.wait_recv()
    o_copies = {}
    for dx in (2, 1, 3, 0):
        chip = lax.rem(x + dx, XN)
        rows = pl.ds(pl.multiple_of(chip * 160, 160), 160)
        ckeys = cslot[:, 0].reshape(YN * CB, HD)
        cvals = cslot[:, 1].reshape(YN * CB, HD)
        sc = lax.dot_general(qb[rows, :], ckeys, NT_DIMS, preferred_element_type=F32) * factor
        mw_ = mwin[rows, :]
        m = jnp.maximum(jnp.max(sc, axis=1, keepdims=True), mw_)
        p = jnp.concatenate(
            [jnp.exp(sc[:, i * 128 : (i + 1) * 128] - m) for i in range(YN * CB // 128)], axis=1
        )
        alpha = jnp.exp(mw_ - m)
        den = alpha * lwin[rows, :] + jnp.sum(p, axis=1, keepdims=True)
        o = alpha * owin[rows, :] + jnp.dot(p.astype(BF16), cvals, preferred_element_type=F32)
        o = (o / den).astype(BF16)
        attn[2 * dx] = o[0:80]
        attn[2 * dx + 1] = o[80:160]
        for cc in range(2):
            if dx != 0:
                cp = rcopy(
                    attn.at[2 * dx + cc], own.at[2 * dx + c],
                    os_sem.at[2 * dx + cc], or_sem.at[2 * dx + c], s, chip * 2 + cc,
                )
                cp.start()
                o_copies[(dx, cc)] = cp
        if dx == 0:
            cp = rcopy(attn.at[1 - c], own.at[c], os_sem.at[0], or_sem.at[c], s, tp_of(0, 1))
            cp.start()
            o_copies[(0, 1)] = cp
            own[c] = attn[c]

    loads["ow"].wait()
    for n, dx in enumerate((0, 1, 3, 2)):
        for cc in range(2):
            src = own.at[2 * dx + cc]
            if dx == 0:
                if cc == 1:
                    rcopy(
                        attn.at[1 - c], own.at[1 - c], os_sem.at[0], or_sem.at[1 - c], s, tp_of(0, 1)
                    ).wait_recv()
            else:
                rcopy(
                    attn.at[2 * dx + cc], src, os_sem.at[2 * dx + cc], or_sem.at[2 * dx + cc],
                    s, tp_of(dx, 0),
                ).wait_recv()
        lhs = jnp.concatenate([own[2 * dx], own[2 * dx + 1]], axis=1)
        chip = lax.rem(x + XN - dx, XN)
        wrows = pl.ds(pl.multiple_of(chip * 256, 256), 256)
        res = pl.ds(pl.multiple_of(t * 80, 80), 80)
        for q in range(8):
            cols = slice(q * 256, (q + 1) * 256)
            o = jnp.dot(lhs, wo[wrows, cols], preferred_element_type=F32)
            if n > 0:
                o += acc[:, cols]
            if n < 3:
                acc[:, cols] = o
            else:
                for i in range(2):
                    j = 2 * q + i
                    jc = slice(j * 128, (j + 1) * 128)
                    v = lat[res, jc].astype(F32) + mrow(4, j) * o[:, i * 128 : (i + 1) * 128]
                    out_ref[:, jc] = v.astype(BF16)

    a_copy.wait_send()
    f_copy.wait_send()
    for cp in (*z_copies, *b_copies, *y_copies, *o_copies.values()):
        cp.wait_send()

    @pl.when(has_next)
    def _():
        to_next.wait_send()

    @pl.when(has_prev)
    def _():
        to_prev.wait_send()


def shards(
    latents, cond, ctx_cond, context, norm_gain, shift_weight, scale_weight, gate_weight,
    q_weight, k_weight, v_weight, out_weight, rel_bias,
):
    dma = pltpu.SemaphoreType.DMA
    scratch = [
        pltpu.VMEM((TOK, D), BF16),
        pltpu.VMEM((NT, 128), F32),
        pltpu.VMEM((NT, 128), F32),
        pltpu.VMEM((ZN, CR, D), BF16),
        pltpu.VMEM((NT, 128), F32),
        pltpu.VMEM((3, 256, D), BF16),
        pltpu.VMEM((D, 384), BF16),
        pltpu.VMEM((1024, D), BF16),
        pltpu.VMEM((1, 15, 31), F32),
        pltpu.VMEM((2, 5, 8, 128), F32),
        pltpu.VMEM((5, 8, 128), F32),
        pltpu.VMEM((XN, 2, 5, 8, 128), F32),
        pltpu.VMEM((2, 5, 8, 128), F32),
        pltpu.VMEM((TOK, 128), F32),
        pltpu.VMEM((2, 15, 128), F32),
        pltpu.VMEM((14, GW, 128), F32),
        pltpu.VMEM((TOK + CB, D), BF16),
        pltpu.VMEM((TOK, HD), BF16),
        pltpu.VMEM((2, KVN, HD), BF16),
        pltpu.VMEM((2, CB, HD), BF16),
        pltpu.VMEM((YN, 2, CB, HD), BF16),
        pltpu.VMEM((TOK, HD), F32),
        pltpu.VMEM((TOK, HD), F32),
        pltpu.VMEM((TOK, HD), F32),
        pltpu.VMEM((8, 80, HD), BF16),
        pltpu.VMEM((8, 80, HD), BF16),
        pltpu.VMEM((80, D), F32),
        dma((13,)), dma((2,)), dma((8,)), dma((8,)), dma((ZN,)), dma((ZN,)), dma((2,)),
        dma((YN,)), dma((YN,)), dma((4,)), dma((8,)), dma((8,)),
    ]
    anyspec = pl.BlockSpec(memory_space=pl.ANY)
    return pl.pallas_call(
        body,
        out_shape=jax.ShapeDtypeStruct((80, D), BF16),
        in_specs=[anyspec] * 13,
        out_specs=pl.BlockSpec(memory_space=pltpu.VMEM),
        scratch_shapes=scratch,
        compiler_params=pltpu.CompilerParams(
            collective_id=0, has_side_effects=True, vmem_limit_bytes=56 * 1024 * 1024
        ),
        name="step",
    )(
        latents, cond.reshape(NT, 128), ctx_cond.reshape(NT, 128), context, norm_gain.reshape(NT, 128),
        shift_weight, scale_weight, gate_weight, q_weight, k_weight, v_weight, out_weight, rel_bias,
    )


def solution(mesh):
    in_specs = (
        P("sp", None),
        P(),
        P(),
        P("sp", None),
        P(),
        P("tp", None),
        P("tp", None),
        P("tp", None),
        P(None, "tp"),
        P(None, "tp"),
        P(None, "tp"),
        P(),
        P("tp", None, None),
    )
    out_specs = P(("sp", "tp"), None)
    return jax.shard_map(shards, mesh=mesh, in_specs=in_specs, out_specs=out_specs, check_vma=False)
```

time: 140 us -> 51.9 us (0.37)
  blocking collectives: 58.6 us -> 0 us
  Pallas kernels: 0 us -> 48.7 us
  starting transfers between devices: 38.7 us -> 0 us
  matrix products: 15.6 us -> 0 us
  local copies, waits for them, and re-layouts: 12.6 us -> 3.01 us
  other arithmetic: 7.76 us -> 0 us
  waiting for transfers between devices: 5.56 us -> 0 us
    all_gather x1 -> x0, blocking collectives: 58.6 us -> none  [sent_together(): whole = lax.all_gather(both, axis, axis=dim, tiled=True)]
    pallas_call x0 -> x1, Pallas kernels: none -> 48.7 us  [shards(): pl.pallas_call(body, out_shape=jax.ShapeDtypeStruct((80, D), BF16), in_sp...]
    all_to_all x2 -> x0, starting transfers between devices: 36.2 us -> none  [the longest x1 22.3 us: shards(): lax.all_to_all(attn, 'tp', split_axis=0, concat_axis=1, tiled=True)]
    dot_general x15 -> x0, matrix products: 15.6 us -> none  [the longest x1 3.83 us: shards(): mixed = jnp.dot(own_rows, out_weight, preferred_element_type=jnp.float32)]
    all_to_all x2 -> x0, waiting for transfers between devices: 5.55 us -> none  [the longest x1 5.55 us: shards(): lax.all_to_all(attn, 'tp', split_axis=0, concat_axis=1, tiled=True)]
    gather x2 -> x0, local copies, waits for them, and re-layouts: 4.84 us -> none  [shards(): padded[:, local_index]]
    convert_element_type x2 -> x0, other arithmetic: 3.76 us -> none  [the longest x1 2.83 us: modulated_norm(): (rows_f * inverse * gain * (1.0 + scale_row) + shift_row).astype(jnp.bflo...]
    reduce_sum x5 -> x0, other arithmetic: 3.65 us -> none  [the longest x2 2.45 us: modulated_norm(): inverse = lax.rsqrt(jnp.mean(rows_f * rows_f, axis=-1, keepdims=True) + EPS)]
  transfers between devices with their start and end apart: 4 -> 0, of which waited for: 1 -> 0; matrix products, arithmetic and copies ran while one was open for 9% -> 0% of each run, Pallas kernels for 0% -> 0%
where the time goes in v1:
time: 51.9 us; the launch traced here: 51.7 us
  Pallas kernels  48.7 us (94%)
  local copies, waits for them, and re-layouts  3.01 us (6%)
    pallas_call x1, Pallas kernels, shards(): pl.pallas_call(body, out_shape=jax.ShapeDtypeStruct((80, D), BF16), in_sp...  48.7 us
    unnamed x2, local copies, waits for them, and re-layouts  3.01 us

profile of v1, /device:TPU:1, one launch (start us, length us, event | category | flops | bytes accessed | tf_op | source)
XLA Modules:
  0.0 51.7 jit_solution(13187787309256254640)
XLA Ops:
  0.0 1.3 %copy.14.rb_h = f32[1,15,31]{2,1,0:T(8,128)} copy(f32[1,15,31]{2,0,1:T(1,128)} %param.25) | data formatting | bytes 3720 | tf_op args[12]
  1.3 48.7 %step.1 = bf16[80,2048]{1,0:T(8,128)(2,1)} custom-call(bf16[640,2048]{1,0:T(8,128)(2,1)} %lat_h.1, f32[16,128]{1,0:T(8,128)} %bitcast.3, f32[16,128]{1,0:T(8,128)} %bitcast.4, bf16[8,2048]{1,0:T(8,128)(2,1)} %ctx_h.1, f32[16,128]{1,0:T(8,128)} %bitcast.5, bf16[256,2048]{1,0:T(8,128)(2,1)} %shw_h.1, bf16[256,2048]{1,0:T(8,128)(2,1)} %scw_h.1, ...), custom_call_target="tpu_custom_call" | custom-call | tf_op jit(solution)/shard_map/step/pallas_call | solution.py:413
  50.0 1.7 %copy.16 = bf16[80,2048]{1,0:T(8,128)(2,1)} copy(bf16[80,2048]{1,0:T(8,128)(2,1)} %step.1) | data formatting | bytes 655360

commit v2 on v1

v2 whole, which is shorter than its diff:
```python
import jax
import jax.numpy as jnp
from jax import lax
from jax.experimental import pallas as pl
from jax.experimental.pallas import tpu as pltpu
from jax.sharding import PartitionSpec as P

D = 2048
HD = 128
GW = 64
WR = 8
WC = 16
EPS = 1e-06
NEG = -1e30
ZN, YN, XN = 12, 8, 4
NT = D // 128
TOK = 640
ROWS = TOK // GW
ALL_ROWS = ROWS * ZN * YN
BEFORE, AFTER = 4, 3
OWN = BEFORE * GW
KVN = (BEFORE + ROWS + AFTER) * GW
CR = 8
NEAR = (0, 1, 2, 3, 4, 11, 10, 9)
FAR = (5, 6, 7, 8)
NB, FB = CR * len(NEAR), CR * len(FAR)
F32 = jnp.float32
BF16 = jnp.bfloat16
NT_DIMS = (((1,), (1,)), ((), ()))


def body(
    lat_h, cond_h, cctx_h, ctx_h, gain_h, shw_h, scw_h, gtw_h, qw_h, kw_h, vw_h, ow_h, rb_h,
    out_ref,
    lat, cond, cctx, craw, gain, mw, w, wo, rb,
    part, recva, red, mod, inv, bias, hbuf, qb, kv, kown, farin, kvn, kvf,
    mwin, lwin, owin, attn, own, acc,
    in_sem, a_sem, bs_sem, br_sem, zs_sem, zr_sem, f_sem, ys_sem, yr_sem, ws_sem, wr_sem, vs_sem, vr_sem, far_sem, h_sem, os_sem, or_sem,
):
    s = lax.axis_index("sp")
    t = lax.axis_index("tp")
    z, y = s // YN, s % YN
    x, c = t // 2, t % 2

    def tp_of(dx, f):
        return lax.rem(x + dx, XN) * 2 + (c if f == 0 else 1 - c)

    tp_peers = [(dx, f) for dx in (2, 1, 3, 0) for f in (0, 1) if (dx, f) != (0, 0)]
    def by_hops(offsets):
        return sorted(offsets, key=lambda d: -min(d, ZN - d))

    raw_order = by_hops((-o) % ZN for o in NEAR[1:])
    far_order = by_hops((-o) % ZN for o in FAR)
    meet_order = by_hops((1, 2, 3, 4, 8, 9, 10, 11))
    y_order = sorted(range(1, YN), key=lambda d: -min(d, YN - d))

    scope = []

    def phase(name):
        while scope:
            scope.pop().__exit__(None, None, None)
        if name:
            scope.append(jax.named_scope(name))
            scope[0].__enter__()

    barrier = pltpu.get_barrier_semaphore()

    def hello(sp, tp):
        pl.semaphore_signal(
            barrier, inc=1, device_id={"sp": sp, "tp": tp}, device_id_type=pl.DeviceIdType.MESH
        )

    def sp_z(d):
        return lax.rem(z + d, ZN) * YN + y

    def sp_y(d):
        return z * YN + lax.rem(y + d, YN)

    for d in meet_order:
        hello(sp_z(d), t)
    for d in y_order:
        hello(sp_y(d), t)
    for dx, f in tp_peers:
        hello(s, tp_of(dx, f))
    has_next = s < ZN * YN - 1
    has_prev = s > 0
    next_far = jnp.logical_and(y == YN - 1, has_next)
    prev_far = jnp.logical_and(y == 0, has_prev)

    @pl.when(next_far)
    def _():
        hello(s + 1, t)

    @pl.when(prev_far)
    def _():
        hello(s - 1, t)

    loads = {}

    def load(name, k, src, dst):
        loads[name] = pltpu.make_async_copy(src, dst, in_sem.at[k])
        loads[name].start()

    load("ctx", 5, ctx_h, craw.at[0])
    load("cond", 0, cond_h, cond)
    load("cctx", 1, cctx_h, cctx)
    load("sc", 2, scw_h, mw.at[0])
    load("sh", 3, shw_h, mw.at[1])
    load("rb", 6, rb_h, rb)
    load("gain", 7, gain_h, gain)
    load("gt", 4, gtw_h, mw.at[2])
    load("lat", 8, lat_h, lat)
    load("qw", 9, qw_h, w.at[:, 0:128])
    load("kw", 10, kw_h, w.at[:, 128:256])
    load("vw", 11, vw_h, w.at[:, 256:384])
    load("ow", 12, ow_h, wo)

    def rcopy(src, dst, ssem, rsem, sp, tp):
        return pltpu.make_async_remote_copy(
            src_ref=src, dst_ref=dst, send_sem=ssem, recv_sem=rsem,
            device_id={"sp": sp, "tp": tp}, device_id_type=pl.DeviceIdType.MESH,
        )

    loads["cond"].wait()
    loads["cctx"].wait()

    def silu_row(ref):
        v = jnp.concatenate([ref[pl.ds(2 * t, 1), :], ref[pl.ds(2 * t + 1, 1), :]], axis=1)
        return (v / (1.0 + jnp.exp(-v))).astype(BF16)

    half = pl.ds(pl.multiple_of(c * 1024, 1024), 1024)
    z_copies = [
        rcopy(
            craw.at[0, :, half], craw.at[NEAR.index(ZN - d), :, half], zs_sem.at[d], zr_sem.at[ZN - d],
            sp_z(d), t,
        )
        for d in raw_order
    ]

    def meet():
        with jax.named_scope("meet"):
            loads["ctx"].wait()
            pl.semaphore_wait(
                barrier,
                len(meet_order) + YN - 1 + 2 * XN - 1 + next_far.astype(jnp.int32) + prev_far.astype(jnp.int32),
            )
            for cp in z_copies:
                cp.start()
            for i, d in enumerate((3, ZN - 3)):
                pl.semaphore_signal(
                    far_sem.at[i], inc=1, device_id={"sp": sp_z(d), "tp": t},
                    device_id_type=pl.DeviceIdType.MESH,
                )

    late = jnp.logical_and(z >= 7, y >= 4)

    @pl.when(late)
    def _():
        meet()

    def act_rows():
        row = lax.broadcasted_iota(jnp.int32, (16, 256), 0)
        return jnp.where(
            row == 0,
            silu_row(cond).astype(F32),
            jnp.where(row == 1, silu_row(cctx).astype(F32), 0.0),
        ).astype(BF16)

    def partial(k, name):
        act = act_rows()
        loads[name].wait()
        for n in range(8):
            o = jnp.dot(act, mw[k, :, n * 256 : (n + 1) * 256], preferred_element_type=F32)
            for i in range(2):
                j = 2 * n + i
                piece = o[:, i * 128 : (i + 1) * 128]
                for r in range(1 if k == 2 else 2):
                    part[j // 8, 2 * k + r, j % 8 : j % 8 + 1, :] = piece[r : r + 1, :]

    with jax.named_scope("partials"):
        partial(0, "sc")
        partial(1, "sh")

    @pl.when(jnp.logical_not(late))
    def _():
        meet()

    vec, gate = slice(0, 4), slice(4, 5)
    a_copy = rcopy(part.at[1 - c, vec], recva.at[vec], a_sem.at[0], a_sem.at[1], s, tp_of(0, 1))
    g_copy = rcopy(part.at[1 - c, gate], recva.at[gate], a_sem.at[2], a_sem.at[3], s, tp_of(0, 1))
    a_copy.start()
    with jax.named_scope("gatepart"):
        partial(2, "gt")
    g_copy.start()
    with jax.named_scope("await_a"):
        a_copy.wait_recv()
    red[0, 0, vec] = part[c, vec] + recva[vec]
    b_copies = [
        rcopy(
            red.at[0, 0, vec], red.at[dx, f, vec], bs_sem.at[2 * dx + f], br_sem.at[2 * dx + f],
            s, tp_of(dx, f),
        )
        for dx, f in tp_peers
    ]
    g_copies = [
        rcopy(
            red.at[0, 0, gate], red.at[dx, f, gate], bs_sem.at[8 + 2 * dx + f],
            br_sem.at[8 + 2 * dx + f], s, tp_of(dx, f),
        )
        for dx, f in tp_peers
    ]
    for cp in b_copies:
        cp.start()

    phase("bias")
    loads["rb"].wait()
    rb_rows = [jnp.concatenate([rb[a], jnp.zeros((1, 97), F32)], axis=1) for a in range(15)]
    lane = lax.broadcasted_iota(jnp.int32, (1, 128), 1)
    qcol = lax.broadcasted_iota(jnp.int32, (GW, 128), 0)
    kcol = lax.broadcasted_iota(jnp.int32, (GW, 128), 1) % GW
    first = jnp.clip(qcol - WC // 2, 0, GW - WC)
    inside = jnp.logical_and(kcol >= first, kcol < first + WC)
    for a in range(14):
        v = jnp.where(
            jnp.logical_and(lane >= 49, lane <= 79),
            pltpu.roll(rb_rows[a + 1], 49, 1),
            pltpu.roll(rb_rows[a], 113, 1),
        )
        spread = pltpu.roll(jnp.broadcast_to(v, (GW, 128)), 0, 1, stride=1, stride_axis=0)
        bias[a] = jnp.where(inside, spread, NEG)

    phase("rms")
    loads["lat"].wait()
    for b in range(TOK // 128):
        rows = slice(b * 128, (b + 1) * 128)
        sq = jnp.zeros((128, 128), F32)
        for j in range(NT):
            v = lat[rows, j * 128 : (j + 1) * 128].astype(F32)
            sq += v * v
        mean = jnp.sum(sq, axis=1, keepdims=True) * (1.0 / D)
        inv[rows, :] = jnp.broadcast_to(lax.rsqrt(mean + EPS), (128, 128))

    phase("send_g")
    g_copy.wait_recv()
    red[0, 0, gate] = part[c, gate] + recva[gate]
    for cp in g_copies:
        cp.start()
    with jax.named_scope("await_b"):
        for cp in b_copies:
            cp.wait_recv()
    loads["gain"].wait()
    for f in range(2):
        tot = red[0, f, vec] + red[1, f, vec] + red[2, f, vec] + red[3, f, vec]
        hh = c if f == 0 else 1 - c
        gn = gain[pl.ds(pl.multiple_of(hh * 8, 8), 8), :]
        mod[hh, 0] = gn * (1.0 + tot[0])
        mod[hh, 1] = gn * (1.0 + tot[1])
        mod[hh, 2] = tot[2]
        mod[hh, 3] = tot[3]

    def mrow(v, j):
        return mod[j // 8, v, j % 8 : j % 8 + 1, :]

    for name in ("qw", "kw", "vw"):
        loads[name].wait()

    def project(r0, n):
        rows = slice(r0, r0 + n)
        for j in range(NT):
            cols = slice(j * 128, (j + 1) * 128)
            v = lat[rows, cols].astype(F32) * inv[rows, :] * mrow(0, j) + mrow(2, j)
            hbuf[rows, cols] = v.astype(BF16)
        o = jnp.dot(hbuf[rows, :], w[...], preferred_element_type=F32).astype(BF16)
        qb[rows, :] = o[:, 0:128]
        kv[0, OWN + r0 : OWN + r0 + n, :] = o[:, 128:256]
        kv[1, OWN + r0 : OWN + r0 + n, :] = o[:, 256:384]

    phase("own_kv")
    def ctx_rows(n, at):
        sq = jnp.zeros((n, 128), F32)
        for j in range(NT):
            v = craw[0 : n // CR, :, j * 128 : (j + 1) * 128].astype(F32).reshape(n, 128)
            sq += v * v
        cinv = lax.rsqrt(jnp.sum(sq, axis=1, keepdims=True) * (1.0 / D) + EPS)
        cinv = jnp.broadcast_to(cinv, (n, 128))
        for j in range(NT):
            cols = slice(j * 128, (j + 1) * 128)
            v = craw[0 : n // CR, :, cols].astype(F32).reshape(n, 128)
            hbuf[at : at + n, cols] = (v * cinv * mrow(1, j) + mrow(3, j)).astype(BF16)

    hbuf[TOK + NB : TOK + NB + 16, :] = jnp.zeros((16, D), BF16)
    ctx_rows(CR, TOK + NB)
    o = jnp.dot(hbuf[TOK + NB : TOK + NB + 16, :], w[:, 128:384], preferred_element_type=F32)
    for i in range(2):
        kown[i] = o[0:CR, i * 128 : (i + 1) * 128].astype(BF16)
    for i in range(2):
        pl.semaphore_wait(far_sem.at[i], 1)
    v_copies = [
        rcopy(
            kown, farin.at[FAR.index(ZN - d)], vs_sem.at[FAR.index(ZN - d)],
            vr_sem.at[FAR.index(ZN - d)], sp_z(d), t,
        )
        for d in far_order
    ]
    for cp in v_copies:
        cp.start()

    phase("proj_edge")
    project(TOK - BEFORE * GW, BEFORE * GW)
    to_next = rcopy(
        kv.at[:, KVN - (BEFORE + AFTER) * GW : KVN - AFTER * GW, :], kv.at[:, 0:OWN, :],
        h_sem.at[0], h_sem.at[1], s + 1, t,
    )

    @pl.when(has_next)
    def _():
        to_next.start()

    project(0, BEFORE * GW)
    to_prev = rcopy(
        kv.at[:, OWN : OWN + AFTER * GW, :], kv.at[:, KVN - AFTER * GW : KVN, :],
        h_sem.at[2], h_sem.at[3], s - 1, t,
    )

    @pl.when(has_prev)
    def _():
        to_prev.start()

    phase("fwd")
    with jax.named_scope('await_z'):
        for cp in z_copies:
            cp.wait_recv()
    f_copy = rcopy(
        craw.at[1:, :, half], craw.at[1:, :, half], f_sem.at[0], f_sem.at[1], s, tp_of(0, 1)
    )
    f_copy.start()

    phase("proj_mid")
    project(BEFORE * GW, TOK - 2 * BEFORE * GW)

    factor = HD ** (-0.5)
    base = s * ROWS

    def window(r):
        g = base + r
        first_row = jnp.clip(g - WR // 2, 0, ALL_ROWS - WR)
        a0 = first_row - g + WR - 1
        k0 = pl.multiple_of((first_row - base + BEFORE) * GW, GW)
        rows = slice(r * GW, (r + 1) * GW)
        keys = kv[0, pl.ds(k0, WR * GW), :]
        vals = kv[1, pl.ds(k0, WR * GW), :]
        sc = lax.dot_general(qb[rows, :], keys, NT_DIMS, preferred_element_type=F32) * factor
        sc = jnp.concatenate(
            [sc[:, i * 128 : (i + 1) * 128] + bias[a0 + 2 * i] for i in range(WR // 2)], axis=1
        )
        m = jnp.max(sc, axis=1, keepdims=True)
        p = jnp.exp(sc - m)
        mwin[rows, :] = jnp.broadcast_to(m, (GW, 128))
        lwin[rows, :] = jnp.broadcast_to(jnp.sum(p, axis=1, keepdims=True), (GW, 128))
        owin[rows, :] = jnp.dot(p.astype(BF16), vals, preferred_element_type=F32)

    phase("ctx_kv")
    f_copy.wait_recv()
    ctx_rows(NB, TOK)
    o = jnp.dot(hbuf[TOK : TOK + NB, :], w[:, 128:384], preferred_element_type=F32)
    for i in range(2):
        kvn[0, i] = o[:, i * 128 : (i + 1) * 128].astype(BF16)
    y_copies = [
        rcopy(kvn.at[0], kvn.at[YN - d], ys_sem.at[d], yr_sem.at[YN - d], sp_y(d), t)
        for d in y_order
    ]
    for cp in y_copies:
        cp.start()

    phase("win_mid")
    for r in range(BEFORE, ROWS - AFTER):
        window(r)

    phase("await_halo")

    @pl.when(has_prev)
    def _():
        to_next.wait_recv()

    @pl.when(has_next)
    def _():
        to_prev.wait_recv()

    phase("win_edge")
    for r in (*range(BEFORE), *range(ROWS - AFTER, ROWS)):
        window(r)

    phase("await_far")
    for cp in v_copies:
        cp.wait_recv()
    for i in range(2):
        kvf[0, i] = farin[:, i].astype(F32).reshape(FB, HD).astype(BF16)
    w_copies = [
        rcopy(kvf.at[0], kvf.at[YN - d], ws_sem.at[d], wr_sem.at[YN - d], sp_y(d), t)
        for d in y_order
    ]
    for cp in w_copies:
        cp.start()

    def merge(rows, ctx):
        ckeys = ctx[:, 0].reshape(-1, HD)
        cvals = ctx[:, 1].reshape(-1, HD)
        sc = lax.dot_general(qb[rows, :], ckeys, NT_DIMS, preferred_element_type=F32) * factor
        m0 = mwin[rows, :]
        m = jnp.maximum(jnp.max(sc, axis=1, keepdims=True), m0)
        p = jnp.concatenate(
            [jnp.exp(sc[:, i * 128 : (i + 1) * 128] - m) for i in range(sc.shape[1] // 128)], axis=1
        )
        alpha = jnp.exp(m0 - m)
        den = alpha * lwin[rows, :] + jnp.sum(p, axis=1, keepdims=True)
        o = alpha * owin[rows, :] + jnp.dot(p.astype(BF16), cvals, preferred_element_type=F32)
        return m, den, o

    phase("await_y")
    for cp in y_copies:
        cp.wait_recv()
    phase("ctx_near")
    for b in range(4):
        rows = slice(b * 160, (b + 1) * 160)
        mwin[rows, :], lwin[rows, :], owin[rows, :] = merge(rows, kvn)
    phase("await_w")
    for cp in w_copies:
        cp.wait_recv()
    phase("ctx_attn")
    o_copies = {}
    for dx in (2, 1, 3, 0):
        chip = lax.rem(x + dx, XN)
        rows = pl.ds(pl.multiple_of(chip * 160, 160), 160)
        _, den, o = merge(rows, kvf)
        o = (o / den).astype(BF16)
        attn[2 * dx] = o[0:80]
        attn[2 * dx + 1] = o[80:160]
        for cc in range(2):
            if dx != 0:
                cp = rcopy(
                    attn.at[2 * dx + cc], own.at[2 * dx + c],
                    os_sem.at[2 * dx + cc], or_sem.at[2 * dx + c], s, chip * 2 + cc,
                )
                cp.start()
                o_copies[(dx, cc)] = cp
        if dx == 0:
            cp = rcopy(attn.at[1 - c], own.at[c], os_sem.at[0], or_sem.at[c], s, tp_of(0, 1))
            cp.start()
            o_copies[(0, 1)] = cp
            own[c] = attn[c]

    phase("out_proj")
    with jax.named_scope("await_g"):
        for cp in g_copies:
            cp.wait_recv()
    for f in range(2):
        hh = c if f == 0 else 1 - c
        mod[hh, 4] = red[0, f, 4] + red[1, f, 4] + red[2, f, 4] + red[3, f, 4]
    loads["ow"].wait()
    for n, dx in enumerate((0, 1, 3, 2)):
        for cc in range(2):
            src = own.at[2 * dx + cc]
            if dx == 0:
                if cc == 1:
                    rcopy(
                        attn.at[1 - c], own.at[1 - c], os_sem.at[0], or_sem.at[1 - c], s, tp_of(0, 1)
                    ).wait_recv()
            else:
                rcopy(
                    attn.at[2 * dx + cc], src, os_sem.at[2 * dx + cc], or_sem.at[2 * dx + cc],
                    s, tp_of(dx, 0),
                ).wait_recv()
        lhs = jnp.concatenate([own[2 * dx], own[2 * dx + 1]], axis=1)
        chip = lax.rem(x + XN - dx, XN)
        wrows = pl.ds(pl.multiple_of(chip * 256, 256), 256)
        res = pl.ds(pl.multiple_of(t * 80, 80), 80)
        for q in range(8):
            cols = slice(q * 256, (q + 1) * 256)
            o = jnp.dot(lhs, wo[wrows, cols], preferred_element_type=F32)
            if n > 0:
                o += acc[:, cols]
            if n < 3:
                acc[:, cols] = o
            else:
                for i in range(2):
                    j = 2 * q + i
                    jc = slice(j * 128, (j + 1) * 128)
                    v = lat[res, jc].astype(F32) + mrow(4, j) * o[:, i * 128 : (i + 1) * 128]
                    out_ref[:, jc] = v.astype(BF16)

    phase("drain")
    a_copy.wait_send()
    f_copy.wait_send()
    g_copy.wait_send()
    for cp in (*z_copies, *b_copies, *g_copies, *v_copies, *y_copies, *w_copies, *o_copies.values()):
        cp.wait_send()

    @pl.when(has_next)
    def _():
        to_next.wait_send()

    @pl.when(has_prev)
    def _():
        to_prev.wait_send()

    phase(None)


def shards(
    latents, cond, ctx_cond, context, norm_gain, shift_weight, scale_weight, gate_weight,
    q_weight, k_weight, v_weight, out_weight, rel_bias,
):
    dma = pltpu.SemaphoreType.DMA
    scratch = [
        pltpu.VMEM((TOK, D), BF16),
        pltpu.VMEM((NT, 128), F32),
        pltpu.VMEM((NT, 128), F32),
        pltpu.VMEM((len(NEAR), CR, D), BF16),
        pltpu.VMEM((NT, 128), F32),
        pltpu.VMEM((3, 256, D), BF16),
        pltpu.VMEM((D, 384), BF16),
        pltpu.VMEM((1024, D), BF16),
        pltpu.VMEM((15, 1, 31), F32),
        pltpu.VMEM((2, 5, 8, 128), F32),
        pltpu.VMEM((5, 8, 128), F32),
        pltpu.VMEM((XN, 2, 5, 8, 128), F32),
        pltpu.VMEM((2, 5, 8, 128), F32),
        pltpu.VMEM((TOK, 128), F32),
        pltpu.VMEM((14, GW, 128), F32),
        pltpu.VMEM((TOK + NB + 16, D), BF16),
        pltpu.VMEM((TOK, HD), BF16),
        pltpu.VMEM((2, KVN, HD), BF16),
        pltpu.VMEM((2, CR, HD), BF16),
        pltpu.VMEM((len(FAR), 2, CR, HD), BF16),
        pltpu.VMEM((YN, 2, NB, HD), BF16),
        pltpu.VMEM((YN, 2, FB, HD), BF16),
        pltpu.VMEM((TOK, HD), F32),
        pltpu.VMEM((TOK, HD), F32),
        pltpu.VMEM((TOK, HD), F32),
        pltpu.VMEM((8, 80, HD), BF16),
        pltpu.VMEM((8, 80, HD), BF16),
        pltpu.VMEM((80, D), F32),
        dma((13,)), dma((4,)), dma((16,)), dma((16,)), dma((ZN,)), dma((ZN,)), dma((2,)),
        dma((YN,)), dma((YN,)), dma((YN,)), dma((YN,)), dma((4,)), dma((4,)),
        pltpu.SemaphoreType.REGULAR((2,)), dma((4,)), dma((8,)), dma((8,)),
    ]
    anyspec = pl.BlockSpec(memory_space=pl.ANY)
    operands = (
        latents, cond.reshape(NT, 128), ctx_cond.reshape(NT, 128), context, norm_gain.reshape(NT, 128),
        shift_weight, scale_weight, gate_weight, q_weight, k_weight, v_weight, out_weight,
        rel_bias.transpose(1, 0, 2),
    )
    return pl.pallas_call(
        body,
        out_shape=jax.ShapeDtypeStruct((80, D), BF16),
        in_specs=[anyspec] * len(operands),
        out_specs=pl.BlockSpec(memory_space=pltpu.VMEM),
        scratch_shapes=scratch,
        compiler_params=pltpu.CompilerParams(
            collective_id=0, has_side_effects=True, vmem_limit_bytes=40 * 1024 * 1024
        ),
        name="step",
    )(*(pltpu.with_memory_space_constraint(v, pltpu.HBM) for v in operands))


def solution(mesh):
    in_specs = (
        P("sp", None),
        P(),
        P(),
        P("sp", None),
        P(),
        P("tp", None),
        P("tp", None),
        P("tp", None),
        P(None, "tp"),
        P(None, "tp"),
        P(None, "tp"),
        P(),
        P("tp", None, None),
    )
    out_specs = P(("sp", "tp"), None)
    return jax.shard_map(shards, mesh=mesh, in_specs=in_specs, out_specs=out_specs, check_vma=False)
```

time: 51.9 us -> 45 us (0.87)
  Pallas kernels: 48.7 us -> 44.1 us
  local copies, waits for them, and re-layouts: 3.01 us -> 0.73 us
    pallas_call x1, Pallas kernels: 48.7 us -> 44.1 us  [shards(): pl.pallas_call(body, out_shape=jax.ShapeDtypeStruct((80, D), BF16), in_sp...]
    unnamed x2 -> x1, local copies, waits for them, and re-layouts: 3.01 us -> 0.73 us
where the time goes in v2:
time: 45 us; the launch traced here: 44.9 us
  Pallas kernels  44.1 us (98%)
  local copies, waits for them, and re-layouts  0.73 us (2%)
    pallas_call x1, Pallas kernels, shards(): pl.pallas_call(body, out_shape=jax.ShapeDtypeStruct((80, D), BF16), in_sp...  44.1 us

profile of v2, /device:TPU:1, one launch (start us, length us, event | category | flops | bytes accessed | tf_op | source)
XLA Modules:
  0.0 44.9 jit_solution(12050220881894725554)
XLA Ops:
  0.0 44.1 %step.1 = bf16[80,2048]{1,0:T(8,128)(2,1)S(1)} custom-call(bf16[640,2048]{1,0:T(8,128)(2,1)} %lat_h.1, f32[16,128]{1,0:T(8,128)} %bitcast.4, f32[16,128]{1,0:T(8,128)} %bitcast.5, bf16[8,2048]{1,0:T(8,128)(2,1)} %ctx_h.1, f32[16,128]{1,0:T(8,128)} %bitcast.6, bf16[256,2048]{1,0:T(8,128)(2,1)} %shw_h.1, bf16[256,2048]{1,0:T(8,128)(2,1)} %scw_h.1, ...), custom_call_target="tpu_custom_call" | custom-call | tf_op jit(solution)/shard_map/step/pallas_call | solution.py:553
  44.1 0.7 %copy.15 = bf16[80,2048]{1,0:T(8,128)(2,1)} copy(bf16[80,2048]{1,0:T(8,128)(2,1)S(1)} %step.1) | data formatting | bytes 655360

commit v3 on v2

--- a/solution.py
+++ b/solution.py
@@ -24,6 +24,8 @@
 NEAR = (0, 1, 2, 3, 4, 11, 10, 9)
 FAR = (5, 6, 7, 8)
 NB, FB = CR * len(NEAR), CR * len(FAR)
+YH = YN // 2
+ZB = CR * YH
 F32 = jnp.float32
 BF16 = jnp.bfloat16
 NT_DIMS = (((1,), (1,)), ((), ()))
@@ -33,14 +35,17 @@
     lat_h, cond_h, cctx_h, ctx_h, gain_h, shw_h, scw_h, gtw_h, qw_h, kw_h, vw_h, ow_h, rb_h,
     out_ref,
     lat, cond, cctx, craw, gain, mw, w, wo, rb,
-    part, recva, red, mod, inv, bias, hbuf, qb, kv, kown, farin, kvn, kvf,
+    part, recva, red, redg, mod, inv, bias, hbuf, qb, kv, kown, farin, kvn, kvf, kvz, yraw,
     mwin, lwin, owin, attn, own, acc,
-    in_sem, a_sem, bs_sem, br_sem, zs_sem, zr_sem, f_sem, ys_sem, yr_sem, ws_sem, wr_sem, vs_sem, vr_sem, far_sem, h_sem, os_sem, or_sem,
+    in_sem, a_sem, b_sem, z_sem, f_sem, ys_sem, yr_sem, ws_sem, wr_sem, v_sem, far_sem, u_sem, ur_sem,
+    fs_sem, fr_sem, k_sem, h_sem, o_sem, or_sem,
 ):
     s = lax.axis_index("sp")
     t = lax.axis_index("tp")
     z, y = s // YN, s % YN
     x, c = t // 2, t % 2
+    yi = y // 2
+    even, odd = y % 2 == 0, y % 2 == 1
 
     def tp_of(dx, f):
         return lax.rem(x + dx, XN) * 2 + (c if f == 0 else 1 - c)
@@ -63,6 +68,7 @@
             scope.append(jax.named_scope(name))
             scope[0].__enter__()
 
+    phase("hello")
     barrier = pltpu.get_barrier_semaphore()
 
     def hello(sp, tp):
@@ -102,6 +108,12 @@
         loads[name].start()
 
     load("ctx", 5, ctx_h, craw.at[0])
+    own_row = pltpu.make_async_copy(ctx_h, yraw.at[yi], in_sem.at[13])
+
+    @pl.when(even)
+    def _():
+        own_row.start()
+
     load("cond", 0, cond_h, cond)
     load("cctx", 1, cctx_h, cctx)
     load("sc", 2, scw_h, mw.at[0])
@@ -121,9 +133,6 @@
             device_id={"sp": sp, "tp": tp}, device_id_type=pl.DeviceIdType.MESH,
         )
 
-    loads["cond"].wait()
-    loads["cctx"].wait()
-
     def silu_row(ref):
         v = jnp.concatenate([ref[pl.ds(2 * t, 1), :], ref[pl.ds(2 * t + 1, 1), :]], axis=1)
         return (v / (1.0 + jnp.exp(-v))).astype(BF16)
@@ -131,11 +140,19 @@
     half = pl.ds(pl.multiple_of(c * 1024, 1024), 1024)
     z_copies = [
         rcopy(
-            craw.at[0, :, half], craw.at[NEAR.index(ZN - d), :, half], zs_sem.at[d], zr_sem.at[ZN - d],
+            craw.at[0, :, half], craw.at[NEAR.index(ZN - d), :, half], z_sem.at[0], z_sem.at[1],
             sp_z(d), t,
         )
         for d in raw_order
     ]
+
+    y_raw = [
+        rcopy(craw.at[0, :, half], yraw.at[yi, :, half], u_sem.at[0], ur_sem.at[yi], sp_y(d), t)
+        for d in y_order
+    ]
+
+    def arrived(ref, sem, i):
+        return rcopy(ref, ref, u_sem.at[0], sem.at[i], sp_y(1), t)
 
     def meet():
         with jax.named_scope("meet"):
@@ -144,8 +161,17 @@
                 barrier,
                 len(meet_order) + YN - 1 + 2 * XN - 1 + next_far.astype(jnp.int32) + prev_far.astype(jnp.int32),
             )
-            for cp in z_copies:
-                cp.start()
+
+            @pl.when(odd)
+            def _():
+                for cp in z_copies:
+                    cp.start()
+
+            @pl.when(even)
+            def _():
+                for cp in y_raw:
+                    cp.start()
+
             for i, d in enumerate((3, ZN - 3)):
                 pl.semaphore_signal(
                     far_sem.at[i], inc=1, device_id={"sp": sp_z(d), "tp": t},
@@ -178,6 +204,8 @@
                     part[j // 8, 2 * k + r, j % 8 : j % 8 + 1, :] = piece[r : r + 1, :]
 
     with jax.named_scope("partials"):
+        loads["cond"].wait()
+        loads["cctx"].wait()
         partial(0, "sc")
         partial(1, "sh")
 
@@ -194,23 +222,32 @@
     g_copy.start()
     with jax.named_scope("await_a"):
         a_copy.wait_recv()
-    red[0, 0, vec] = part[c, vec] + recva[vec]
+    red[0] = (part[c, vec] + recva[vec]).astype(BF16)
     b_copies = [
         rcopy(
-            red.at[0, 0, vec], red.at[dx, f, vec], bs_sem.at[2 * dx + f], br_sem.at[2 * dx + f],
-            s, tp_of(dx, f),
+            red.at[0], red.at[2 * dx + f], b_sem.at[0], b_sem.at[1], s, tp_of(dx, f),
         )
         for dx, f in tp_peers
     ]
     g_copies = [
         rcopy(
-            red.at[0, 0, gate], red.at[dx, f, gate], bs_sem.at[8 + 2 * dx + f],
-            br_sem.at[8 + 2 * dx + f], s, tp_of(dx, f),
+            redg.at[0], redg.at[2 * dx + f], b_sem.at[2], b_sem.at[3], s, tp_of(dx, f),
         )
         for dx, f in tp_peers
     ]
     for cp in b_copies:
         cp.start()
+
+    def together(ref, sems):
+        return rcopy(ref, ref, sems.at[0], sems.at[1], s, tp_of(0, 1))
+
+    b_all = together(red.at[1:], b_sem.at[0:2])
+    g_all = together(redg.at[1:], b_sem.at[2:4])
+    z_all = together(craw.at[1:, :, half], z_sem)
+    u_all = together(craw.at[1:, :, half], u_sem)
+    v_all = together(farin, v_sem)
+    k_all = together(kvz.at[1:], k_sem)
+    o_all = together(attn.at[1:], o_sem)
 
     phase("bias")
     loads["rb"].wait()
@@ -242,15 +279,14 @@
 
     phase("send_g")
     g_copy.wait_recv()
-    red[0, 0, gate] = part[c, gate] + recva[gate]
+    redg[0] = part[c, 4] + recva[4]
     for cp in g_copies:
         cp.start()
     with jax.named_scope("await_b"):
-        for cp in b_copies:
-            cp.wait_recv()
+        b_all.wait_recv()
     loads["gain"].wait()
     for f in range(2):
-        tot = red[0, f, vec] + red[1, f, vec] + red[2, f, vec] + red[3, f, vec]
+        tot = sum(red[2 * k + f].astype(F32) for k in range(XN))
         hh = c if f == 0 else 1 - c
         gn = gain[pl.ds(pl.multiple_of(hh * 8, 8), 8), :]
         mod[hh, 0] = gn * (1.0 + tot[0])
@@ -276,34 +312,38 @@
         kv[1, OWN + r0 : OWN + r0 + n, :] = o[:, 256:384]
 
     phase("own_kv")
-    def ctx_rows(n, at):
+    for i in range(2):
+        pl.semaphore_wait(far_sem.at[i], 1)
+
+    def ctx_rows(ref, n, at):
         sq = jnp.zeros((n, 128), F32)
         for j in range(NT):
-            v = craw[0 : n // CR, :, j * 128 : (j + 1) * 128].astype(F32).reshape(n, 128)
+            v = ref[0 : n // CR, :, j * 128 : (j + 1) * 128].astype(F32).reshape(n, 128)
             sq += v * v
         cinv = lax.rsqrt(jnp.sum(sq, axis=1, keepdims=True) * (1.0 / D) + EPS)
         cinv = jnp.broadcast_to(cinv, (n, 128))
         for j in range(NT):
             cols = slice(j * 128, (j + 1) * 128)
-            v = craw[0 : n // CR, :, cols].astype(F32).reshape(n, 128)
+            v = ref[0 : n // CR, :, cols].astype(F32).reshape(n, 128)
             hbuf[at : at + n, cols] = (v * cinv * mrow(1, j) + mrow(3, j)).astype(BF16)
 
-    hbuf[TOK + NB : TOK + NB + 16, :] = jnp.zeros((16, D), BF16)
-    ctx_rows(CR, TOK + NB)
-    o = jnp.dot(hbuf[TOK + NB : TOK + NB + 16, :], w[:, 128:384], preferred_element_type=F32)
-    for i in range(2):
-        kown[i] = o[0:CR, i * 128 : (i + 1) * 128].astype(BF16)
-    for i in range(2):
-        pl.semaphore_wait(far_sem.at[i], 1)
     v_copies = [
         rcopy(
-            kown, farin.at[FAR.index(ZN - d)], vs_sem.at[FAR.index(ZN - d)],
-            vr_sem.at[FAR.index(ZN - d)], sp_z(d), t,
+            kown, farin.at[FAR.index(ZN - d)], v_sem.at[0], v_sem.at[1], sp_z(d), t,
         )
         for d in far_order
     ]
-    for cp in v_copies:
-        cp.start()
+
+    @pl.when(odd)
+    def _():
+        at = TOK + NB
+        hbuf[at : at + 16, :] = jnp.zeros((16, D), BF16)
+        ctx_rows(craw, CR, at)
+        o = jnp.dot(hbuf[at : at + 16, :], w[:, 128:384], preferred_element_type=F32)
+        for i in range(2):
+            kown[i] = o[0:CR, i * 128 : (i + 1) * 128].astype(BF16)
+        for cp in v_copies:
+            cp.start()
 
     phase("proj_edge")
     project(TOK - BEFORE * GW, BEFORE * GW)
@@ -316,6 +356,27 @@
     def _():
         to_next.start()
 
+    phase("fwd")
+    fy_copies = [
+        rcopy(yraw.at[i, :, half], yraw.at[i, :, half], fs_sem.at[i], fr_sem.at[i], s, tp_of(0, 1))
+        for i in range(YH)
+    ]
+    f_copy = rcopy(
+        craw.at[1:, :, half], craw.at[1:, :, half], f_sem.at[0], f_sem.at[1], s, tp_of(0, 1)
+    )
+    for i in range(YH):
+
+        @pl.when(y != 2 * i)
+        def _():
+            arrived(yraw.at[i, :, half], ur_sem, i).wait_recv()
+            fy_copies[i].start()
+
+    @pl.when(odd)
+    def _():
+        z_all.wait_recv()
+        f_copy.start()
+
+    phase("proj_first")
     project(0, BEFORE * GW)
     to_prev = rcopy(
         kv.at[:, OWN : OWN + AFTER * GW, :], kv.at[:, KVN - AFTER * GW : KVN, :],
@@ -326,14 +387,46 @@
     def _():
         to_prev.start()
 
-    phase("fwd")
-    with jax.named_scope('await_z'):
-        for cp in z_copies:
-            cp.wait_recv()
-    f_copy = rcopy(
-        craw.at[1:, :, half], craw.at[1:, :, half], f_sem.at[0], f_sem.at[1], s, tp_of(0, 1)
-    )
-    f_copy.start()
+    phase("ctx_z")
+    @pl.when(even)
+    def _():
+        own_row.wait()
+
+    for i in range(YH):
+
+        @pl.when(y != 2 * i)
+        def _():
+            fy_copies[i].wait_recv()
+
+    at = TOK + NB + 16
+    ctx_rows(yraw, ZB, at)
+    o = jnp.dot(hbuf[at : at + ZB, :], w[:, 128:384], preferred_element_type=F32)
+    for i in range(2):
+        kvz[0, i] = o[:, i * 128 : (i + 1) * 128].astype(BF16)
+    k_copies = [
+        rcopy(kvz.at[0], kvz.at[ZN - d], k_sem.at[0], k_sem.at[1], sp_z(d), t)
+        for d in by_hops(range(1, ZN))
+    ]
+    for cp in k_copies:
+        cp.start()
+
+    phase("ctx_kv")
+    y_copies = [
+        rcopy(kvn.at[yi], kvn.at[yi], ys_sem.at[d], yr_sem.at[yi], sp_y(d), t) for d in y_order
+    ]
+    w_copies = [
+        rcopy(kvf.at[yi], kvf.at[yi], ws_sem.at[d], wr_sem.at[yi], sp_y(d), t) for d in y_order
+    ]
+
+    @pl.when(odd)
+    def _():
+        f_copy.wait_recv()
+        ctx_rows(craw, NB, TOK)
+        o = jnp.dot(hbuf[TOK : TOK + NB, :], w[:, 128:384], preferred_element_type=F32)
+        for i in range(2):
+            kvn[yi, i] = o[:, i * 128 : (i + 1) * 128].astype(BF16)
+        for cp in y_copies:
+            cp.start()
 
     phase("proj_mid")
     project(BEFORE * GW, TOK - 2 * BEFORE * GW)
@@ -359,23 +452,20 @@
         lwin[rows, :] = jnp.broadcast_to(jnp.sum(p, axis=1, keepdims=True), (GW, 128))
         owin[rows, :] = jnp.dot(p.astype(BF16), vals, preferred_element_type=F32)
 
-    phase("ctx_kv")
-    f_copy.wait_recv()
-    ctx_rows(NB, TOK)
-    o = jnp.dot(hbuf[TOK : TOK + NB, :], w[:, 128:384], preferred_element_type=F32)
-    for i in range(2):
-        kvn[0, i] = o[:, i * 128 : (i + 1) * 128].astype(BF16)
-    y_copies = [
-        rcopy(kvn.at[0], kvn.at[YN - d], ys_sem.at[d], yr_sem.at[YN - d], sp_y(d), t)
-        for d in y_order
-    ]
-    for cp in y_copies:
-        cp.start()
-
     phase("win_mid")
     for r in range(BEFORE, ROWS - AFTER):
         window(r)
 
+    phase("await_far")
+
+    @pl.when(odd)
+    def _():
+        v_all.wait_recv()
+        for i in range(2):
+            kvf[yi, i] = farin[:, i].astype(F32).reshape(FB, HD).astype(BF16)
+        for cp in w_copies:
+            cp.start()
+
     phase("await_halo")
 
     @pl.when(has_prev)
@@ -390,86 +480,82 @@
     for r in (*range(BEFORE), *range(ROWS - AFTER, ROWS)):
         window(r)
 
-    phase("await_far")
-    for cp in v_copies:
-        cp.wait_recv()
-    for i in range(2):
-        kvf[0, i] = farin[:, i].astype(F32).reshape(FB, HD).astype(BF16)
-    w_copies = [
-        rcopy(kvf.at[0], kvf.at[YN - d], ws_sem.at[d], wr_sem.at[YN - d], sp_y(d), t)
-        for d in y_order
-    ]
-    for cp in w_copies:
-        cp.start()
-
-    def merge(rows, ctx):
-        ckeys = ctx[:, 0].reshape(-1, HD)
-        cvals = ctx[:, 1].reshape(-1, HD)
-        sc = lax.dot_general(qb[rows, :], ckeys, NT_DIMS, preferred_element_type=F32) * factor
+    def merge(rows, parts):
+        q = qb[rows, :]
+        scs = []
+        for ctx in parts:
+            keys = ctx[:, 0].reshape(-1, HD)
+            sc = lax.dot_general(q, keys, NT_DIMS, preferred_element_type=F32) * factor
+            scs.append(sc)
         m0 = mwin[rows, :]
-        m = jnp.maximum(jnp.max(sc, axis=1, keepdims=True), m0)
-        p = jnp.concatenate(
-            [jnp.exp(sc[:, i * 128 : (i + 1) * 128] - m) for i in range(sc.shape[1] // 128)], axis=1
-        )
+        m = m0
+        for sc in scs:
+            m = jnp.maximum(m, jnp.max(sc, axis=1, keepdims=True))
         alpha = jnp.exp(m0 - m)
-        den = alpha * lwin[rows, :] + jnp.sum(p, axis=1, keepdims=True)
-        o = alpha * owin[rows, :] + jnp.dot(p.astype(BF16), cvals, preferred_element_type=F32)
+        den = alpha * lwin[rows, :]
+        o = alpha * owin[rows, :]
+        for ctx, sc in zip(parts, scs):
+            vals = ctx[:, 1].reshape(-1, HD)
+            p = jnp.concatenate(
+                [jnp.exp(sc[:, i * 128 : (i + 1) * 128] - m) for i in range(sc.shape[1] // 128)],
+                axis=1,
+            )
+            den += jnp.sum(p, axis=1, keepdims=True)
+            o += jnp.dot(p.astype(BF16), vals, preferred_element_type=F32)
         return m, den, o
 
     phase("await_y")
-    for cp in y_copies:
-        cp.wait_recv()
+    for i in range(YH):
+
+        @pl.when(y != 2 * i + 1)
+        def _():
+            arrived(kvn.at[i], yr_sem, i).wait_recv()
+
     phase("ctx_near")
     for b in range(4):
         rows = slice(b * 160, (b + 1) * 160)
-        mwin[rows, :], lwin[rows, :], owin[rows, :] = merge(rows, kvn)
-    phase("await_w")
-    for cp in w_copies:
-        cp.wait_recv()
+        mwin[rows, :], lwin[rows, :], owin[rows, :] = merge(rows, (kvn,))
+    phase("await_k")
+    for i in range(YH):
+
+        @pl.when(y != 2 * i + 1)
+        def _():
+            arrived(kvf.at[i], wr_sem, i).wait_recv()
+
+    phase("await_k2")
+    k_all.wait_recv()
     phase("ctx_attn")
-    o_copies = {}
-    for dx in (2, 1, 3, 0):
-        chip = lax.rem(x + dx, XN)
-        rows = pl.ds(pl.multiple_of(chip * 160, 160), 160)
-        _, den, o = merge(rows, kvf)
-        o = (o / den).astype(BF16)
-        attn[2 * dx] = o[0:80]
-        attn[2 * dx + 1] = o[80:160]
-        for cc in range(2):
-            if dx != 0:
-                cp = rcopy(
-                    attn.at[2 * dx + cc], own.at[2 * dx + c],
-                    os_sem.at[2 * dx + cc], or_sem.at[2 * dx + c], s, chip * 2 + cc,
-                )
-                cp.start()
-                o_copies[(dx, cc)] = cp
-        if dx == 0:
-            cp = rcopy(attn.at[1 - c], own.at[c], os_sem.at[0], or_sem.at[c], s, tp_of(0, 1))
-            cp.start()
-            o_copies[(0, 1)] = cp
-            own[c] = attn[c]
+    for pair in ((2, 1), (3, 0)):
+        done = []
+        for dx in pair:
+            chip = lax.rem(x + dx, XN)
+            _, den, o = merge(pl.ds(pl.multiple_of(chip * 160, 160), 160), (kvf, kvz))
+            done.append((o / den).astype(BF16))
+        for dx, o in zip(pair, done):
+            attn[2 * dx] = o[0:80]
+            attn[2 * dx + 1] = o[80:160]
+        for dx in pair:
+            chip = lax.rem(x + dx, XN)
+            if dx == 0:
+                rcopy(attn.at[1 - c], own.at[c], o_sem.at[0], or_sem.at[0], s, tp_of(0, 1)).start()
+                own[c] = attn[c]
+                continue
+            for cc in range(2):
+                rcopy(
+                    attn.at[2 * dx + cc], own.at[2 * dx + c], o_sem.at[0], or_sem.at[dx],
+                    s, chip * 2 + cc,
+                ).start()
 
     phase("out_proj")
     with jax.named_scope("await_g"):
-        for cp in g_copies:
-            cp.wait_recv()
+        g_all.wait_recv()
     for f in range(2):
         hh = c if f == 0 else 1 - c
-        mod[hh, 4] = red[0, f, 4] + red[1, f, 4] + red[2, f, 4] + red[3, f, 4]
+        mod[hh, 4] = redg[f] + redg[2 + f] + redg[4 + f] + redg[6 + f]
     loads["ow"].wait()
     for n, dx in enumerate((0, 1, 3, 2)):
-        for cc in range(2):
-            src = own.at[2 * dx + cc]
-            if dx == 0:
-                if cc == 1:
-                    rcopy(
-                        attn.at[1 - c], own.at[1 - c], os_sem.at[0], or_sem.at[1 - c], s, tp_of(0, 1)
-                    ).wait_recv()
-            else:
-                rcopy(
-                    attn.at[2 * dx + cc], src, os_sem.at[2 * dx + cc], or_sem.at[2 * dx + cc],
-                    s, tp_of(dx, 0),
-                ).wait_recv()
+        got = own.at[1 - c] if dx == 0 else own.at[2 * dx : 2 * dx + 2]
+        rcopy(got, got, o_sem.at[0], or_sem.at[dx], s, tp_of(0, 1)).wait_recv()
         lhs = jnp.concatenate([own[2 * dx], own[2 * dx + 1]], axis=1)
         chip = lax.rem(x + XN - dx, XN)
         wrows = pl.ds(pl.multiple_of(chip * 256, 256), 256)
@@ -489,11 +575,23 @@
                     out_ref[:, jc] = v.astype(BF16)
 
     phase("drain")
-    a_copy.wait_send()
-    f_copy.wait_send()
-    g_copy.wait_send()
-    for cp in (*z_copies, *b_copies, *g_copies, *v_copies, *y_copies, *w_copies, *o_copies.values()):
+    for cp in (a_copy, g_copy, b_all, g_all, k_all, o_all):
         cp.wait_send()
+
+    @pl.when(odd)
+    def _():
+        for cp in (f_copy, z_all, v_all, *y_copies, *w_copies):
+            cp.wait_send()
+
+    @pl.when(even)
+    def _():
+        u_all.wait_send()
+
+    for i in range(YH):
+
+        @pl.when(y != 2 * i)
+        def _():
+            fy_copies[i].wait_send()
 
     @pl.when(has_next)
     def _():
@@ -523,26 +621,29 @@
         pltpu.VMEM((15, 1, 31), F32),
         pltpu.VMEM((2, 5, 8, 128), F32),
         pltpu.VMEM((5, 8, 128), F32),
-        pltpu.VMEM((XN, 2, 5, 8, 128), F32),
+        pltpu.VMEM((2 * XN, 4, 8, 128), BF16),
+        pltpu.VMEM((2 * XN, 8, 128), F32),
         pltpu.VMEM((2, 5, 8, 128), F32),
         pltpu.VMEM((TOK, 128), F32),
         pltpu.VMEM((14, GW, 128), F32),
-        pltpu.VMEM((TOK + NB + 16, D), BF16),
+        pltpu.VMEM((TOK + NB + 16 + ZB, D), BF16),
         pltpu.VMEM((TOK, HD), BF16),
         pltpu.VMEM((2, KVN, HD), BF16),
         pltpu.VMEM((2, CR, HD), BF16),
         pltpu.VMEM((len(FAR), 2, CR, HD), BF16),
-        pltpu.VMEM((YN, 2, NB, HD), BF16),
-        pltpu.VMEM((YN, 2, FB, HD), BF16),
+        pltpu.VMEM((YH, 2, NB, HD), BF16),
+        pltpu.VMEM((YH, 2, FB, HD), BF16),
+        pltpu.VMEM((ZN, 2, ZB, HD), BF16),
+        pltpu.VMEM((YH, CR, D), BF16),
         pltpu.VMEM((TOK, HD), F32),
         pltpu.VMEM((TOK, HD), F32),
         pltpu.VMEM((TOK, HD), F32),
         pltpu.VMEM((8, 80, HD), BF16),
         pltpu.VMEM((8, 80, HD), BF16),
         pltpu.VMEM((80, D), F32),
-        dma((13,)), dma((4,)), dma((16,)), dma((16,)), dma((ZN,)), dma((ZN,)), dma((2,)),
-        dma((YN,)), dma((YN,)), dma((YN,)), dma((YN,)), dma((4,)), dma((4,)),
-        pltpu.SemaphoreType.REGULAR((2,)), dma((4,)), dma((8,)), dma((8,)),
+        dma((14,)), dma((4,)), dma((4,)), dma((2,)), dma((2,)), dma((YN,)), dma((YH,)), dma((YN,)),
+        dma((YH,)), dma((2,)), pltpu.SemaphoreType.REGULAR((2,)), dma((2,)), dma((YH,)), dma((YH,)),
+        dma((YH,)), dma((2,)), dma((4,)), dma((2,)), dma((XN,)),
     ]
     anyspec = pl.BlockSpec(memory_space=pl.ANY)
     operands = (

time: 45 us -> 42.5 us (0.944)
  Pallas kernels: 44.1 us -> 41.6 us
    pallas_call x1, Pallas kernels: 44.1 us -> 41.6 us  [shards(): pl.pallas_call(body, out_shape=jax.ShapeDtypeStruct((80, D), BF16), in_sp...]
where the time goes in v3:
time: 42.5 us; the launch traced here: 42.3 us
  Pallas kernels  41.6 us (98%)
  local copies, waits for them, and re-layouts  0.73 us (2%)
    pallas_call x1, Pallas kernels, shards(): pl.pallas_call(body, out_shape=jax.ShapeDtypeStruct((80, D), BF16), in_sp...  41.6 us

profile of v3, /device:TPU:1, one launch (start us, length us, event | category | flops | bytes accessed | tf_op | source)
XLA Modules:
  0.0 42.3 jit_solution(849898695989187398)
XLA Ops:
  0.0 41.6 %step.1 = bf16[80,2048]{1,0:T(8,128)(2,1)S(1)} custom-call(bf16[640,2048]{1,0:T(8,128)(2,1)} %lat_h.1, f32[16,128]{1,0:T(8,128)} %bitcast.4, f32[16,128]{1,0:T(8,128)} %bitcast.5, bf16[8,2048]{1,0:T(8,128)(2,1)} %ctx_h.1, f32[16,128]{1,0:T(8,128)} %bitcast.6, bf16[256,2048]{1,0:T(8,128)(2,1)} %shw_h.1, bf16[256,2048]{1,0:T(8,128)(2,1)} %scw_h.1, ...), custom_call_target="tpu_custom_call" | custom-call | tf_op jit(solution)/shard_map/step/pallas_call | solution.py:654
  41.6 0.7 %copy.15 = bf16[80,2048]{1,0:T(8,128)(2,1)} copy(bf16[80,2048]{1,0:T(8,128)(2,1)S(1)} %step.1) | data formatting | bytes 655360

commit v4 on v3

--- a/solution.py
+++ b/solution.py
@@ -34,10 +34,10 @@
 def body(
     lat_h, cond_h, cctx_h, ctx_h, gain_h, shw_h, scw_h, gtw_h, qw_h, kw_h, vw_h, ow_h, rb_h,
     out_ref,
-    lat, cond, cctx, craw, gain, mw, w, wo, rb,
+    lat, cond, craw, gain, mw, w, wo, rb,
     part, recva, red, redg, mod, inv, bias, hbuf, qb, kv, kown, farin, kvn, kvf, kvz, yraw,
     mwin, lwin, owin, attn, own, acc,
-    in_sem, a_sem, b_sem, z_sem, f_sem, ys_sem, yr_sem, ws_sem, wr_sem, v_sem, far_sem, u_sem, ur_sem,
+    in_sem, a_sem, b_sem, z_sem, f_sem, y_sem, yr_sem, wr_sem, v_sem, far_sem, u_sem, ur_sem,
     fs_sem, fr_sem, k_sem, h_sem, o_sem, or_sem,
 ):
     s = lax.axis_index("sp")
@@ -108,14 +108,14 @@
         loads[name].start()
 
     load("ctx", 5, ctx_h, craw.at[0])
-    own_row = pltpu.make_async_copy(ctx_h, yraw.at[yi], in_sem.at[13])
+    own_row = pltpu.make_async_copy(ctx_h, yraw.at[yi], in_sem.at[1])
 
     @pl.when(even)
     def _():
         own_row.start()
 
-    load("cond", 0, cond_h, cond)
-    load("cctx", 1, cctx_h, cctx)
+    load("cond", 0, cond_h, cond.at[0])
+    load("cctx", 0, cctx_h, cond.at[1])
     load("sc", 2, scw_h, mw.at[0])
     load("sh", 3, shw_h, mw.at[1])
     load("rb", 6, rb_h, rb)
@@ -123,9 +123,9 @@
     load("gt", 4, gtw_h, mw.at[2])
     load("lat", 8, lat_h, lat)
     load("qw", 9, qw_h, w.at[:, 0:128])
-    load("kw", 10, kw_h, w.at[:, 128:256])
-    load("vw", 11, vw_h, w.at[:, 256:384])
-    load("ow", 12, ow_h, wo)
+    load("kw", 9, kw_h, w.at[:, 128:256])
+    load("vw", 9, vw_h, w.at[:, 256:384])
+    load("ow", 10, ow_h, wo)
 
     def rcopy(src, dst, ssem, rsem, sp, tp):
         return pltpu.make_async_remote_copy(
@@ -188,8 +188,8 @@
         row = lax.broadcasted_iota(jnp.int32, (16, 256), 0)
         return jnp.where(
             row == 0,
-            silu_row(cond).astype(F32),
-            jnp.where(row == 1, silu_row(cctx).astype(F32), 0.0),
+            silu_row(cond.at[0]).astype(F32),
+            jnp.where(row == 1, silu_row(cond.at[1]).astype(F32), 0.0),
         ).astype(BF16)
 
     def partial(k, name):
@@ -204,8 +204,7 @@
                     part[j // 8, 2 * k + r, j % 8 : j % 8 + 1, :] = piece[r : r + 1, :]
 
     with jax.named_scope("partials"):
-        loads["cond"].wait()
-        loads["cctx"].wait()
+        pltpu.make_async_copy(cond, cond, in_sem.at[0]).wait()
         partial(0, "sc")
         partial(1, "sh")
 
@@ -248,6 +247,8 @@
     v_all = together(farin, v_sem)
     k_all = together(kvz.at[1:], k_sem)
     o_all = together(attn.at[1:], o_sem)
+    y_all = together(kvn.at[1:], y_sem)
+    w_all = rcopy(kvf.at[1:], kvf.at[1:], y_sem.at[1], y_sem.at[0], s, tp_of(0, 1))
 
     phase("bias")
     loads["rb"].wait()
@@ -297,8 +298,7 @@
     def mrow(v, j):
         return mod[j // 8, v, j % 8 : j % 8 + 1, :]
 
-    for name in ("qw", "kw", "vw"):
-        loads[name].wait()
+    pltpu.make_async_copy(w, w, in_sem.at[9]).wait()
 
     def project(r0, n):
         rows = slice(r0, r0 + n)
@@ -412,10 +412,10 @@
 
     phase("ctx_kv")
     y_copies = [
-        rcopy(kvn.at[yi], kvn.at[yi], ys_sem.at[d], yr_sem.at[yi], sp_y(d), t) for d in y_order
+        rcopy(kvn.at[yi], kvn.at[yi], y_sem.at[0], yr_sem.at[yi], sp_y(d), t) for d in y_order
     ]
     w_copies = [
-        rcopy(kvf.at[yi], kvf.at[yi], ws_sem.at[d], wr_sem.at[yi], sp_y(d), t) for d in y_order
+        rcopy(kvf.at[yi], kvf.at[yi], y_sem.at[1], wr_sem.at[yi], sp_y(d), t) for d in y_order
     ]
 
     @pl.when(odd)
@@ -514,7 +514,7 @@
     phase("ctx_near")
     for b in range(4):
         rows = slice(b * 160, (b + 1) * 160)
-        mwin[rows, :], lwin[rows, :], owin[rows, :] = merge(rows, (kvn,))
+        mwin[rows, :], lwin[rows, :], owin[rows, :] = merge(rows, (kvn.at[0:YH],))
     phase("await_k")
     for i in range(YH):
 
@@ -525,11 +525,11 @@
     phase("await_k2")
     k_all.wait_recv()
     phase("ctx_attn")
-    for pair in ((2, 1), (3, 0)):
+    for pair in ((2, 1), (3,), (0,)):
         done = []
         for dx in pair:
             chip = lax.rem(x + dx, XN)
-            _, den, o = merge(pl.ds(pl.multiple_of(chip * 160, 160), 160), (kvf, kvz))
+            _, den, o = merge(pl.ds(pl.multiple_of(chip * 160, 160), 160), (kvf.at[0:YH], kvz))
             done.append((o / den).astype(BF16))
         for dx, o in zip(pair, done):
             attn[2 * dx] = o[0:80]
@@ -580,7 +580,7 @@
 
     @pl.when(odd)
     def _():
-        for cp in (f_copy, z_all, v_all, *y_copies, *w_copies):
+        for cp in (f_copy, z_all, v_all, y_all, w_all):
             cp.wait_send()
 
     @pl.when(even)
@@ -611,8 +611,7 @@
     dma = pltpu.SemaphoreType.DMA
     scratch = [
         pltpu.VMEM((TOK, D), BF16),
-        pltpu.VMEM((NT, 128), F32),
-        pltpu.VMEM((NT, 128), F32),
+        pltpu.VMEM((2, NT, 128), F32),
         pltpu.VMEM((len(NEAR), CR, D), BF16),
         pltpu.VMEM((NT, 128), F32),
         pltpu.VMEM((3, 256, D), BF16),
@@ -631,8 +630,8 @@
         pltpu.VMEM((2, KVN, HD), BF16),
         pltpu.VMEM((2, CR, HD), BF16),
         pltpu.VMEM((len(FAR), 2, CR, HD), BF16),
-        pltpu.VMEM((YH, 2, NB, HD), BF16),
-        pltpu.VMEM((YH, 2, FB, HD), BF16),
+        pltpu.VMEM((YN, 2, NB, HD), BF16),
+        pltpu.VMEM((YN, 2, FB, HD), BF16),
         pltpu.VMEM((ZN, 2, ZB, HD), BF16),
         pltpu.VMEM((YH, CR, D), BF16),
         pltpu.VMEM((TOK, HD), F32),
@@ -641,7 +640,7 @@
         pltpu.VMEM((8, 80, HD), BF16),
         pltpu.VMEM((8, 80, HD), BF16),
         pltpu.VMEM((80, D), F32),
-        dma((14,)), dma((4,)), dma((4,)), dma((2,)), dma((2,)), dma((YN,)), dma((YH,)), dma((YN,)),
+        dma((11,)), dma((4,)), dma((4,)), dma((2,)), dma((2,)), dma((2,)), dma((YH,)),
         dma((YH,)), dma((2,)), pltpu.SemaphoreType.REGULAR((2,)), dma((2,)), dma((YH,)), dma((YH,)),
         dma((YH,)), dma((2,)), dma((4,)), dma((2,)), dma((XN,)),
     ]

time: 42.5 us -> 42.3 us (level)
  no operation moved by 1% of the time
where the time goes in v4:
time: 42.3 us; the launch traced here: 42.2 us
  Pallas kernels  41.4 us (98%)
  local copies, waits for them, and re-layouts  0.73 us (2%)
    pallas_call x1, Pallas kernels, shards(): pl.pallas_call(body, out_shape=jax.ShapeDtypeStruct((80, D), BF16), in_sp...  41.4 us

profile of v4, /device:TPU:1, one launch (start us, length us, event | category | flops | bytes accessed | tf_op | source)
XLA Modules:
  0.0 42.2 jit_solution(16921414855264100748)
XLA Ops:
  0.0 41.4 %step.1 = bf16[80,2048]{1,0:T(8,128)(2,1)S(1)} custom-call(bf16[640,2048]{1,0:T(8,128)(2,1)} %lat_h.1, f32[16,128]{1,0:T(8,128)} %bitcast.4, f32[16,128]{1,0:T(8,128)} %bitcast.5, bf16[8,2048]{1,0:T(8,128)(2,1)} %ctx_h.1, f32[16,128]{1,0:T(8,128)} %bitcast.6, bf16[256,2048]{1,0:T(8,128)(2,1)} %shw_h.1, bf16[256,2048]{1,0:T(8,128)(2,1)} %scw_h.1, ...), custom_call_target="tpu_custom_call" | custom-call | tf_op jit(solution)/shard_map/step/pallas_call | solution.py:653
  41.4 0.7 %copy.15 = bf16[80,2048]{1,0:T(8,128)(2,1)} copy(bf16[80,2048]{1,0:T(8,128)(2,1)S(1)} %step.1) | data formatting | bytes 655360

commit v5 on v4

--- a/solution.py
+++ b/solution.py
@@ -1,3 +1,5 @@
+import functools
+
 import jax
 import jax.numpy as jnp
 from jax import lax
@@ -488,20 +490,20 @@
             sc = lax.dot_general(q, keys, NT_DIMS, preferred_element_type=F32) * factor
             scs.append(sc)
         m0 = mwin[rows, :]
-        m = m0
-        for sc in scs:
-            m = jnp.maximum(m, jnp.max(sc, axis=1, keepdims=True))
+        tiles = [
+            [sc[:, i * 128 : (i + 1) * 128] for i in range(sc.shape[1] // 128)] for sc in scs
+        ]
+        top = functools.reduce(jnp.maximum, sum(tiles, []))
+        m = jnp.maximum(jnp.max(top, axis=1, keepdims=True), m0)
         alpha = jnp.exp(m0 - m)
-        den = alpha * lwin[rows, :]
+        exps = [[jnp.exp(tile - m) for tile in part] for part in tiles]
+        total = functools.reduce(jnp.add, sum(exps, []))
+        den = alpha * lwin[rows, :] + jnp.sum(total, axis=1, keepdims=True)
         o = alpha * owin[rows, :]
-        for ctx, sc in zip(parts, scs):
+        for ctx, part in zip(parts, exps):
             vals = ctx[:, 1].reshape(-1, HD)
-            p = jnp.concatenate(
-                [jnp.exp(sc[:, i * 128 : (i + 1) * 128] - m) for i in range(sc.shape[1] // 128)],
-                axis=1,
-            )
-            den += jnp.sum(p, axis=1, keepdims=True)
-            o += jnp.dot(p.astype(BF16), vals, preferred_element_type=F32)
+            p = jnp.concatenate(part, axis=1).astype(BF16)
+            o += jnp.dot(p, vals, preferred_element_type=F32)
         return m, den, o
 
     phase("await_y")

time: 42.3 us -> 42.3 us (level)
  no operation moved by 1% of the time
where the time goes in v5:
time: 42.3 us; the launch traced here: 42.2 us
  Pallas kernels  41.4 us (98%)
  local copies, waits for them, and re-layouts  0.73 us (2%)
    pallas_call x1, Pallas kernels, shards(): pl.pallas_call(body, out_shape=jax.ShapeDtypeStruct((80, D), BF16), in_sp...  41.4 us

profile of v5, /device:TPU:1, one launch (start us, length us, event | category | flops | bytes accessed | tf_op | source)
XLA Modules:
  0.0 42.2 jit_solution(18327793141006055894)
XLA Ops:
  0.0 41.4 %step.1 = bf16[80,2048]{1,0:T(8,128)(2,1)S(1)} custom-call(bf16[640,2048]{1,0:T(8,128)(2,1)} %lat_h.1, f32[16,128]{1,0:T(8,128)} %bitcast.4, f32[16,128]{1,0:T(8,128)} %bitcast.5, bf16[8,2048]{1,0:T(8,128)(2,1)} %ctx_h.1, f32[16,128]{1,0:T(8,128)} %bitcast.6, bf16[256,2048]{1,0:T(8,128)(2,1)} %shw_h.1, bf16[256,2048]{1,0:T(8,128)(2,1)} %scw_h.1, ...), custom_call_target="tpu_custom_call" | custom-call | tf_op jit(solution)/shard_map/step/pallas_call | solution.py:655
  41.4 0.7 %copy.15 = bf16[80,2048]{1,0:T(8,128)(2,1)} copy(bf16[80,2048]{1,0:T(8,128)(2,1)S(1)} %step.1) | data formatting | bytes 655360
